TPU v7x, 512 devices: a whole 4x8x8 slice. The times are simulated.
512 devices in a mesh: fs: 64 (over z, y), tp: 8 (over x, core).
Axes of the slice: x: 4, y: 8, z: 8, core: 2. Of those that a mesh axis runs over, the one named last changes fastest.
Arguments:
- prompt: bfloat16 [20480, 2048], P('fs', 'tp'), may hold values from -6 to 6
- norm_gain: float32 [2048], P('fs'), may hold values from 0.1 to 1.9
- gate_master: float32 [2048, 3072], P('fs', 'tp'), may hold values from -0.125 to 0.125
- up_master: float32 [2048, 3072], P('fs', 'tp'), may hold values from -0.125 to 0.125
- down_master: float32 [2048, 3072], P('fs', 'tp'), may hold values from -0.109375 to 0.109375
Outputs:
- gate_new: bfloat16 [3072, 2048], P('tp')
- up_new: bfloat16 [3072, 2048], P('tp')
- down_new: bfloat16 [3072, 2048], P('tp')
- mixed: bfloat16 [2048, 20480], P('tp', 'fs')
All inputs are finite; a program needn't handle non-finite values.
Results may differ from a plain program's by a relative error of at most 0.0082.
Values may be sent and summed in bfloat16 or wider, within the bound.
No kernel may reach another device: no remote copies, remote signals or barrier semaphores. Data moves between devices by JAX's collectives and lax.ppermute only.
A program may use at most 64 MiB of HBM per device.

v0:
```python
import jax
import jax.numpy as jnp
from jax import lax
from jax.sharding import PartitionSpec as P


def laid_out(parts, dim):
    parts = jnp.moveaxis(parts, 0, dim)
    shape = parts.shape
    return parts.reshape(*shape[:dim], shape[dim] * shape[dim + 1], *shape[dim + 2 :])


def sent_to_all(array, axis):
    copies = jnp.broadcast_to(array, (lax.axis_size(axis), *array.shape))
    return lax.all_to_all(copies, axis, split_axis=0, concat_axis=0, tiled=True)


def gathered_copies(array, axis, dim):
    return laid_out(sent_to_all(array, axis), dim)


def gather_turned(arrays, axis, dims):
    turned = [jnp.moveaxis(a, dim, 0) for a, dim in zip(arrays, dims)]
    widths = [t[0].size for t in turned]
    both = jnp.concatenate([t.reshape(-1, w) for t, w in zip(turned, widths)], axis=1)
    filled = lax.all_gather(both, axis, axis=0, tiled=True)
    parts = jnp.split(filled, [sum(widths[:k]) for k in range(1, len(widths))], axis=1)
    return tuple(
        (
            jnp.moveaxis(b.reshape(-1, *t.shape[1:]), 0, dim)
            for b, t, dim in zip(parts, turned, dims)
        )
    )


def cut_along(array, dim, size):
    before, after = (array.shape[:dim], array.shape[dim + 1 :])
    return jnp.moveaxis(array.reshape(*before, size, -1, *after), dim, 0)


def sent_and_summed(array, axis, dim):
    parts = cut_along(array, dim, lax.axis_size(axis))
    arrived = lax.all_to_all(parts, axis, split_axis=0, concat_axis=0, tiled=True)
    return arrived.astype(jnp.float32).sum(axis=0)


def on_device(prompt, norm_gain, gate_master, up_master, down_master):
    gain_col = norm_gain[:, None]
    gate_low = (gate_master * gain_col).astype(jnp.bfloat16).T
    up_low = (up_master * gain_col).astype(jnp.bfloat16).T
    down_low = down_master.astype(jnp.bfloat16).T
    whole = gathered_copies(prompt, "tp", 1)
    values = whole.astype(jnp.float32)
    normed = (values * lax.rsqrt(jnp.mean(values * values, axis=1, keepdims=True) + 1e-06)).astype(
        jnp.bfloat16
    )
    contract = (((1,), (1,)), ((), ()))
    gate_new, up_new, down_new = gather_turned((gate_low, up_low, down_low), "fs", (1, 1, 1))
    gate = lax.dot_general(normed, gate_new, contract, preferred_element_type=jnp.float32)
    up = lax.dot_general(normed, up_new, contract, preferred_element_type=jnp.float32)
    hidden = (jax.nn.silu(gate) * up).astype(jnp.bfloat16)
    mixed = sent_and_summed(
        lax.dot_general(
            down_new, hidden, (((0,), (1,)), ((), ())), preferred_element_type=jnp.float32
        ).astype(jnp.bfloat16),
        "tp",
        0,
    )
    return (gate_new, up_new, down_new, mixed.astype(jnp.bfloat16))


def solution(mesh):
    placed = (P("fs", "tp"), P("fs"), P("fs", "tp"), P("fs", "tp"), P("fs", "tp"))
    return jax.shard_map(
        on_device,
        mesh=mesh,
        in_specs=placed,
        out_specs=(P("tp", None), P("tp", None), P("tp", None), P("tp", "fs")),
        check_vma=False,
    )
```

profile of v0, /device:TPU:1, one launch (start us, length us, event | category | flops | bytes accessed | tf_op | source)
XLA Modules:
  0.0 145.5 jit_solution(8326352939495786494)
XLA Ops:
  7.2 0.0 all-gather.2.cloned.1.call-start
  7.2 0.8 convert_element_type.35
  8.0 0.9 multiply_convert_fusion.2
  8.9 0.6 pad_maximum_fusion
  9.6 0.0 all-gather.2.cloned.1.call-update
  9.6 1.0 broadcast_in_dim.2
  10.6 27.0 %all_to_all.10 = bf16[8,320,256]{2,1,0:T(8,128)(2,1)S(1)} all-to-all(bf16[8,320,256]{2,1,0:T(8,128)(2,1)S(1)} %broadcast_in_dim.2), channel_id=1, replica_groups=mesh['fs'=64,'tp'=8] {'tp'}, dimensions={0} | all-to-all | bytes 2621440 | tf_op jit(solution)/shard_map/all_to_all | solution.py:15
  37.6 0.2 convert_bitcast_fusion
  37.8 0.3 copy.21
  38.2 0.4 fusion
  38.6 61.7 %all-gather.2.cloned.1.call-done = bf16[2048,1152]{1,0:T(8,128)(2,1)} async-done(((bf16[32,1152]{1,0:T(8,128)(2,1)}), bf16[2048,1152]{1,0:T(8,128)(2,1)}) %all-gather.2.cloned.1.call-update) | async-done | bytes 4718608 | tf_op jit(solution)/shard_map/all_gather | solution.py:26
  100.3 2.3 %fusion.4 = f32[320,384]{1,0:T(8,128)S(1)} fusion(bf16[2048,1152]{1,0:T(8,128)(2,1)} %all-gather.2.cloned.1.call-done, f32[320,2048]{1,0:T(8,128)S(1)} %bitcast.14, f32[320]{0:T(512)S(1)} %add_rsqrt_fusion), kind=kOutput, calls=%fused_computation.10 | convolution fusion | flops 504627200 | bytes 4687104 | tf_op jit(solution)/shard_map/dot_general | solution.py:59
  102.6 4.6 %convolution_convert_fusion = bf16[2048,320]{0,1:T(8,128)(2,1)} fusion(bf16[2048,1152]{1,0:T(8,128)(2,1)} %all-gather.2.cloned.1.call-done, f32[320,384]{1,0:T(8,128)S(1)} %fusion.4, f32[320,2048]{1,0:T(8,128)S(1)} %bitcast.15, f32[320]{0:T(512)S(1)} %add_rsqrt_fusion), kind=kOutput, calls=%fused_computation.2 | convolution fusion | flops 1009336320 | bytes 7570688 | tf_op jit(solution)/shard_map/dot_general | solution.py:63
  107.2 2.5 %copy.23 = bf16[40,8,8,256]{3,2,0,1:T(8,128)(2,1)} copy(bf16[40,8,8,256]{3,2,1,0:T(8,128)(2,1)} %bitcast.16) | data formatting | bytes 2621440 | tf_op jit(solution)/shard_map/reshape | solution.py:38
  109.7 8.9 %all-to-all-start.1 = ((bf16[8,256,320]{1,2,0:T(8,128)(2,1)}), bf16[8,256,320]{1,2,0:T(8,128)(2,1)}, u32[]{:S(2)}, u32[]{:S(2)}) async-start(bf16[8,256,320]{1,2,0:T(8,128)(2,1)} %bitcast.13), calls=%async_computation.1 | async-start | bytes 2621440 | tf_op jit(solution)/shard_map/all_to_all | solution.py:43
  118.6 4.0 %slice_bitcast_fusion = (bf16[384,2048]{0,1:T(8,128)(2,1)}, bf16[384,2048]{0,1:T(8,128)(2,1)S(1)}, bf16[384,2048]{0,1:T(8,128)(2,1)S(1)}) fusion(bf16[2048,1152]{1,0:T(8,128)(2,1)} %all-gather.2.cloned.1.call-done), kind=kLoop, calls=%fused_computation.6 | loop fusion | bytes 9437184 | tf_op jit(solution)/shard_map/transpose | solution.py:30
  122.6 2.6 %copy.19 = bf16[384,2048]{1,0:T(8,128)(2,1)} copy(bf16[384,2048]{0,1:T(8,128)(2,1)} %get-tuple-element.8) | data formatting | bytes 3145728
  125.2 1.6 %copy.18 = bf16[384,2048]{1,0:T(8,128)(2,1)} copy(bf16[384,2048]{0,1:T(8,128)(2,1)S(1)} %get-tuple-element.9) | data formatting | bytes 3145728
  126.8 1.6 %copy.17 = bf16[384,2048]{1,0:T(8,128)(2,1)} copy(bf16[384,2048]{0,1:T(8,128)(2,1)S(1)} %get-tuple-element.10) | data formatting | bytes 3145728
  128.4 8.1 %all-to-all-done.1 = bf16[8,256,320]{1,2,0:T(8,128)(2,1)} async-done(((bf16[8,256,320]{1,2,0:T(8,128)(2,1)}), bf16[8,256,320]{1,2,0:T(8,128)(2,1)}, u32[]{:S(2)}, u32[]{:S(2)}) %all-to-all-start.1) | async-done | bytes 1310752 | tf_op jit(solution)/shard_map/all_to_all | solution.py:43
  136.5 2.2 %reduce_sum.22 = bf16[256,320]{0,1:T(8,128)(2,1)} reduce(bf16[8,256,320]{1,2,0:T(8,128)(2,1)} %all-to-all-done.1, bf16[]{:T(256)} %constant.11.clone.1), dimensions={0}, to_apply=%region_1.2 | reduce | flops 573440 | bytes 1474562 | tf_op jit(solution)/shard_map/reduce_sum | solution.py:44
  (1 shorter events, 0.0 us)
Async XLA Ops:
  7.2 93.1 %all-gather.2.cloned.1.call-start = ((), (), s32[]{:S(2)}) async-start(), calls=%async_computation.2 | async-start | bytes 4792320 | tf_op jit(solution)/shard_map/all_gather | solution.py:26
  109.7 26.8 %all-to-all-start.1 = ((bf16[8,256,320]{1,2,0:T(8,128)(2,1)}), bf16[8,256,320]{1,2,0:T(8,128)(2,1)}, u32[]{:S(2)}, u32[]{:S(2)}) async-start(bf16[8,256,320]{1,2,0:T(8,128)(2,1)} %bitcast.13), calls=%async_computation.1 | async-start | bytes 2621440 | tf_op jit(solution)/shard_map/all_to_all | solution.py:43
Sparse Core Ops, SparseCore 0:
  11.6 88.6 all-gather.1
where the time goes:
time: 146 us
  waiting for transfers between devices  69.8 us (48%)
  blocking collectives  27 us (18%)
  between operations  14.1 us (10%)
  local copies, waits for them, and re-layouts  13.7 us (9%)
  starting transfers between devices  8.97 us (6%)
  matrix products  6.86 us (5%)
  other arithmetic  5.16 us (4%)
    all_gather x1, waiting for transfers between devices, gather_turned(): filled = lax.all_gather(both, axis, axis=0, tiled=True)  61.7 us
    all_to_all x1, blocking collectives, sent_to_all(): return lax.all_to_all(copies, axis, split_axis=0, concat_axis=0, tiled=True)  27 us
    all_to_all x1, starting transfers between devices, sent_and_summed(): lax.all_to_all(parts, axis, split_axis=0, concat_axis=0, tiled=True)  8.93 us
    all_to_all x1, waiting for transfers between devices, sent_and_summed(): lax.all_to_all(parts, axis, split_axis=0, concat_axis=0, tiled=True)  8.07 us
    unnamed x3, local copies, waits for them, and re-layouts  5.81 us
    dot_general x1, matrix products, on_device(): lax.dot_general(down_new, hidden, (((0,), (1,)), ((), ())), preferred_ele...  4.58 us
    transpose x1, local copies, waits for them, and re-layouts, gather_turned(): jnp.moveaxis(b.reshape(-1, *t.shape[1:]), 0, dim)  4 us
  transfers between devices with their start and end apart: 2, of which 2 were waited for; matrix products, arithmetic and copies ran while one was open for 8% of the time, Pallas kernels for 0%

commit v1 on v0

v1 whole, which is shorter than its diff:
```python
import jax
import jax.numpy as jnp
from jax import lax
from jax.sharding import PartitionSpec as P

SCALE = 2.0**18


def on_device(prompt, norm_gain, gate_master, up_master, down_master):
    gain_col = norm_gain[:, None]
    parts = [gate_master * gain_col, up_master * gain_col, down_master]
    low = jnp.concatenate([(lax.reduce_precision(p, 8, 7) * SCALE).astype(jnp.float16) for p in parts], axis=1)
    whole = lax.all_to_all(jnp.broadcast_to(prompt, (8, *prompt.shape)), "tp", 0, 0, tiled=True)
    filled = lax.all_gather(low, "fs", axis=0, tiled=True)
    back = (filled.astype(jnp.float32) * (1 / SCALE)).astype(jnp.bfloat16)
    gate_w, up_w, down_w = back[:, :384], back[:, 384:768], back[:, 768:]
    values = whole.transpose(1, 0, 2).reshape(320, 2048).astype(jnp.float32)
    normed = (values * lax.rsqrt(jnp.mean(values * values, axis=1, keepdims=True) + 1e-06)).astype(jnp.bfloat16)
    gate = jnp.dot(normed, gate_w, preferred_element_type=jnp.float32)
    up = jnp.dot(normed, up_w, preferred_element_type=jnp.float32)
    hidden = (jax.nn.silu(gate) * up).astype(jnp.bfloat16)
    partial = lax.dot_general(down_w, hidden, (((1,), (1,)), ((), ())), preferred_element_type=jnp.float32).astype(jnp.bfloat16)
    arrived = lax.all_to_all(partial.reshape(8, 256, 320), "tp", 0, 0, tiled=True)
    mixed = arrived.astype(jnp.float32).sum(axis=0).astype(jnp.bfloat16)
    return gate_w.T, up_w.T, down_w.T, mixed


def solution(mesh):
    placed = (P("fs", "tp"), P("fs"), P("fs", "tp"), P("fs", "tp"), P("fs", "tp"))
    return jax.shard_map(
        on_device,
        mesh=mesh,
        in_specs=placed,
        out_specs=(P("tp", None), P("tp", None), P("tp", None), P("tp", "fs")),
        check_vma=False,
    )
```

time: 146 us -> 113 us (0.77)
  waiting for transfers between devices: 69.8 us -> 8.07 us
  blocking collectives: 27 us -> 49 us
  starting transfers between devices: 8.97 us -> 24.9 us
  between operations: 14.1 us -> 0.74 us
  local copies, waits for them, and re-layouts: 13.7 us -> 16.8 us
    all_gather x1 -> x0, waiting for transfers between devices: 61.7 us -> none  [gather_turned(): filled = lax.all_gather(both, axis, axis=0, tiled=True)]
    all_gather x0 -> x1, blocking collectives: none -> 49 us  [on_device(): filled = lax.all_gather(low, 'fs', axis=0, tiled=True)]
    all_to_all x1 -> x0, blocking collectives: 27 us -> none  [sent_to_all(): return lax.all_to_all(copies, axis, split_axis=0, concat_axis=0, tiled=True)]
    all_to_all x1 -> x2, starting transfers between devices: 8.93 us -> 24.9 us  [the longest x1 14.5 us: on_device(): lax.all_to_all(partial.reshape(8, 256, 320), 'tp', 0, 0, tiled=True)]
    unnamed x3 -> x15, local copies, waits for them, and re-layouts: 5.81 us -> 7.84 us
    convert_element_type x2, other arithmetic: 1.72 us -> 3.29 us  [the longest x1 3.21 us: on_device(): back = (filled.astype(jnp.float32) * (1 / SCALE)).astype(jnp.bfloat16)]
    all_to_all x1 -> x2, waiting for transfers between devices: 8.07 us -> 8.07 us  [the longest x1 8.07 us: on_device(): lax.all_to_all(partial.reshape(8, 256, 320), 'tp', 0, 0, tiled=True)]
  transfers between devices with their start and end apart: 2 -> 2, of which waited for: 2 -> 1; matrix products, arithmetic and copies ran while one was open for 8% -> 12% of each run, Pallas kernels for 0% -> 0%
where the time goes in v1:
time: 113 us; the launch traced here: 112 us
  blocking collectives  49 us (43%)
  starting transfers between devices  24.9 us (22%)
  local copies, waits for them, and re-layouts  16.8 us (15%)
  waiting for transfers between devices  8.07 us (7%)
  matrix products  6.86 us (6%)
  other arithmetic  6.11 us (5%)
    all_gather x1, blocking collectives, on_device(): filled = lax.all_gather(low, 'fs', axis=0, tiled=True)  49 us
    all_to_all x1, starting transfers between devices, on_device(): lax.all_to_all(partial.reshape(8, 256, 320), 'tp', 0, 0, tiled=True)  14.5 us
    all_to_all x1, starting transfers between devices, on_device(): lax.all_to_all(jnp.broadcast_to(prompt, (8, *prompt.shape)), 'tp', 0, 0,...  10.3 us
    all_to_all x1, waiting for transfers between devices, on_device(): lax.all_to_all(partial.reshape(8, 256, 320), 'tp', 0, 0, tiled=True)  8.07 us
    unnamed x15, local copies, waits for them, and re-layouts  7.84 us
    dot_general x1, matrix products, on_device(): lax.dot_general(down_w, hidden, (((1,), (1,)), ((), ())), preferred_eleme...  4.58 us
    transpose x1, local copies, waits for them, and re-layouts, on_device(): return (gate_w.T, up_w.T, down_w.T, mixed)  4 us
    convert_element_type x1, other arithmetic, on_device(): back = (filled.astype(jnp.float32) * (1 / SCALE)).astype(jnp.bfloat16)  3.21 us
  transfers between devices with their start and end apart: 2, of which 1 were waited for; matrix products, arithmetic and copies ran while one was open for 12% of the time, Pallas kernels for 0%

profile of v1, /device:TPU:1, one launch (start us, length us, event | category | flops | bytes accessed | tf_op | source)
XLA Modules:
  0.0 112.5 jit_solution(16767032419472254907)
XLA Ops:
  0.6 0.0 copy-start.5
  0.7 2.1 %broadcast_in_dim.2 = bf16[8,320,256]{2,1,0:T(8,128)(2,1)} broadcast(bf16[320,256]{1,0:T(8,128)(2,1)} %param.5), dimensions={1,2} | broadcast | bytes 1474560 | tf_op jit(solution)/shard_map/broadcast_in_dim | solution.py:13
  2.8 10.3 %all-to-all-start = ((bf16[8,320,256]{2,1,0:T(8,128)(2,1)}), bf16[8,320,256]{2,1,0:T(8,128)(2,1)S(1)}, u32[]{:S(2)}, u32[]{:S(2)}) async-start(bf16[8,320,256]{2,1,0:T(8,128)(2,1)} %broadcast_in_dim.2), calls=%async_computation | async-start | bytes 2621440 | tf_op jit(solution)/shard_map/all_to_all | solution.py:13
  13.1 0.0 copy-done.5
  13.1 0.1 multiply_convert_fusion.4
  13.2 49.0 %all-gather.1 = f16[2048,1152]{1,0:T(8,128)(2,1)S(1)} all-gather(f16[32,1152]{1,0:T(8,128)(2,1)S(1)} %pad_maximum_fusion), channel_id=1, replica_groups=mesh['fs'=64,'tp'=8] {'fs'}, dimensions={0}, use_global_device_ids=true | all-gather | bytes 4792320 | tf_op jit(solution)/shard_map/all_gather | solution.py:14
  62.3 3.2 %multiply_convert_fusion = bf16[2048,1152]{1,0:T(8,128)(2,1)} fusion(f16[2048,1152]{1,0:T(8,128)(2,1)S(1)} %all-gather.1), kind=kLoop, calls=%fused_computation | loop fusion | flops 7077888 | bytes 9437184 | tf_op jit(solution)/shard_map/convert_element_type | solution.py:15
  65.5 0.0 all-to-all-done
  65.5 1.1 copy-done
  66.5 0.2 convert_bitcast_fusion
  66.8 0.0 copy-start.1
  66.8 0.3 copy.21
  67.2 0.9 copy-done.1
  68.1 0.4 fusion
  68.5 2.3 %fusion.4 = f32[320,384]{1,0:T(8,128)S(1)} fusion(bf16[2048,1152]{1,0:T(8,128)(2,1)} %multiply_convert_fusion, f32[320,2048]{1,0:T(8,128)S(1)} %bitcast.14, f32[320]{0:T(512)S(1)} %add_rsqrt_fusion), kind=kOutput, calls=%fused_computation.11 | convolution fusion | flops 504627200 | bytes 4687104 | tf_op jit(solution)/shard_map/dot_general | solution.py:19
  70.8 4.6 %convolution_convert_fusion = bf16[2048,320]{0,1:T(8,128)(2,1)} fusion(bf16[2048,1152]{1,0:T(8,128)(2,1)} %multiply_convert_fusion, f32[320,384]{1,0:T(8,128)S(1)} %fusion.4, f32[320,2048]{1,0:T(8,128)S(1)} %bitcast.15, f32[320]{0:T(512)S(1)} %add_rsqrt_fusion), kind=kOutput, calls=%fused_computation.3 | convolution fusion | flops 1009336320 | bytes 7570688 | tf_op jit(solution)/shard_map/dot_general | solution.py:22
  75.3 2.5 %copy.23 = bf16[40,8,8,256]{3,2,0,1:T(8,128)(2,1)} copy(bf16[40,8,8,256]{3,2,1,0:T(8,128)(2,1)} %bitcast.16) | data formatting | bytes 2621440 | tf_op jit(solution)/shard_map/reshape | solution.py:23
  77.8 14.5 %all-to-all-start.1 = ((bf16[8,256,320]{1,2,0:T(8,128)(2,1)}), bf16[8,256,320]{1,2,0:T(8,128)(2,1)}, u32[]{:S(2)}, u32[]{:S(2)}) async-start(bf16[8,256,320]{1,2,0:T(8,128)(2,1)} %bitcast.13), calls=%async_computation.1 | async-start | bytes 2621440 | tf_op jit(solution)/shard_map/all_to_all | solution.py:23
  92.4 4.0 %slice_bitcast_fusion = (bf16[384,2048]{0,1:T(8,128)(2,1)S(1)}, bf16[384,2048]{0,1:T(8,128)(2,1)S(1)}, bf16[384,2048]{0,1:T(8,128)(2,1)}) fusion(bf16[2048,1152]{1,0:T(8,128)(2,1)} %multiply_convert_fusion), kind=kLoop, calls=%fused_computation.7 | loop fusion | bytes 9437184 | tf_op jit(solution)/shard_map/transpose | solution.py:25
  96.4 2.6 %copy.17 = bf16[384,2048]{1,0:T(8,128)(2,1)} copy(bf16[384,2048]{0,1:T(8,128)(2,1)} %get-tuple-element.10) | data formatting | bytes 3145728
  99.0 1.6 %copy.18 = bf16[384,2048]{1,0:T(8,128)(2,1)} copy(bf16[384,2048]{0,1:T(8,128)(2,1)S(1)} %get-tuple-element.9) | data formatting | bytes 3145728
  100.6 1.6 %copy.19 = bf16[384,2048]{1,0:T(8,128)(2,1)} copy(bf16[384,2048]{0,1:T(8,128)(2,1)S(1)} %get-tuple-element.8) | data formatting | bytes 3145728
  102.2 8.1 %all-to-all-done.1 = bf16[8,256,320]{1,2,0:T(8,128)(2,1)} async-done(((bf16[8,256,320]{1,2,0:T(8,128)(2,1)}), bf16[8,256,320]{1,2,0:T(8,128)(2,1)}, u32[]{:S(2)}, u32[]{:S(2)}) %all-to-all-start.1) | async-done | bytes 1310752 | tf_op jit(solution)/shard_map/all_to_all | solution.py:23
  110.3 2.2 %reduce_sum.22 = bf16[256,320]{0,1:T(8,128)(2,1)} reduce(bf16[8,256,320]{1,2,0:T(8,128)(2,1)} %all-to-all-done.1, bf16[]{:T(256)} %constant.15.clone.1), dimensions={0}, to_apply=%region_1.2 | reduce | flops 573440 | bytes 1474562 | tf_op jit(solution)/shard_map/reduce_sum | solution.py:24
  (9 shorter events, 0.0 us)
Async XLA Ops:
  0.6 12.5 %copy-start.5 = (f32[32]{0:T(128)S(1)}, f32[32]{0:T(128)}, u32[]{:S(2)}) copy-start(f32[32]{0:T(128)} %param.6) | copy-start | bytes 388
  0.6 12.4 %copy-start.2 = (f32[32,384]{1,0:T(8,128)S(1)}, f32[32,384]{1,0:T(8,128)}, u32[]{:S(2)}) copy-start(f32[32,384]{1,0:T(8,128)} %param.7) | copy-start | bytes 147460
  0.7 12.4 %copy-start.3 = (f32[32,384]{1,0:T(8,128)S(1)}, f32[32,384]{1,0:T(8,128)}, u32[]{:S(2)}) copy-start(f32[32,384]{1,0:T(8,128)} %param.8) | copy-start | bytes 147460
  0.7 12.4 %copy-start.4 = (f32[32,384]{1,0:T(8,128)S(1)}, f32[32,384]{1,0:T(8,128)}, u32[]{:S(2)}) copy-start(f32[32,384]{1,0:T(8,128)} %param.9) | copy-start | bytes 147460
  2.8 62.7 %all-to-all-start = ((bf16[8,320,256]{2,1,0:T(8,128)(2,1)}), bf16[8,320,256]{2,1,0:T(8,128)(2,1)S(1)}, u32[]{:S(2)}, u32[]{:S(2)}) async-start(bf16[8,320,256]{2,1,0:T(8,128)(2,1)} %broadcast_in_dim.2), calls=%async_computation | async-start | bytes 2621440 | tf_op jit(solution)/shard_map/all_to_all | solution.py:13
  65.5 1.1 copy-start
  66.8 1.3 %copy-start.1 = (bf16[8,320,256]{2,1,0:T(8,128)(2,1)S(1)}, bf16[8,320,256]{2,1,0:T(8,128)(2,1)}, u32[]{:S(2)}) copy-start(bf16[8,320,256]{2,1,0:T(8,128)(2,1)} %copy-done) | copy-start | bytes 3932164
  77.8 32.4 %all-to-all-start.1 = ((bf16[8,256,320]{1,2,0:T(8,128)(2,1)}), bf16[8,256,320]{1,2,0:T(8,128)(2,1)}, u32[]{:S(2)}, u32[]{:S(2)}) async-start(bf16[8,256,320]{1,2,0:T(8,128)(2,1)} %bitcast.13), calls=%async_computation.1 | async-start | bytes 2621440 | tf_op jit(solution)/shard_map/all_to_all | solution.py:23

commit v2 on v1

v2 whole, which is shorter than its diff:
```python
import jax
import jax.numpy as jnp
from jax import lax
from jax.experimental import pallas as pl
from jax.experimental.pallas import tpu as pltpu
from jax.sharding import PartitionSpec as P

SIDE = 8
SCALE = 2.0**18
VMEM = pl.BlockSpec(memory_space=pltpu.VMEM)
FAR = pl.BlockSpec(memory_space=pltpu.HBM)
SMEM = pl.BlockSpec(memory_space=pltpu.SMEM)


def struct(shape, dtype=jnp.bfloat16):
    return jax.ShapeDtypeStruct(shape, dtype)


def hidden_kernel(core, x_ref, near_ref, other_ref, mine_ref, kept_ref, low_ref, normed_ref, sems, keep_sem):
    slabs, tokens, width = x_ref.shape
    cols = low_ref.shape[1] // 3
    rows = low_ref.shape[0] // (SIDE * SIDE)
    outer, inner = jnp.where(core[0] == 0, SIDE, 1), jnp.where(core[0] == 0, 1, SIDE)
    copies = []
    for z in range(SIDE):
        for y in range(SIDE):
            row = pl.multiple_of((z * outer + y * inner) * rows, rows)
            to = low_ref.at[pl.ds((z * SIDE + y) * rows, rows)]
            copies.append(pltpu.make_async_copy(near_ref.at[pl.ds(row, rows)], to, sems.at[z, y]))
            copies[-1].start()
    squares = jnp.zeros((tokens, width), jnp.float32)
    for s in range(slabs):
        x = x_ref[s].astype(jnp.float32)
        squares += x * x
    inverse = lax.rsqrt(jnp.sum(squares, axis=1, keepdims=True) / (slabs * width) + 1e-06)
    for s in range(slabs):
        normed_ref[:, s * width : (s + 1) * width] = (x_ref[s].astype(jnp.float32) * inverse).astype(jnp.bfloat16)
    for copy in copies:
        copy.wait()
    keep = pltpu.make_async_copy(low_ref, kept_ref, keep_sem)
    keep.start()
    gate = jnp.dot(normed_ref[...], low_ref[:, :cols], preferred_element_type=jnp.float32)
    up = jnp.dot(normed_ref[...], low_ref[:, cols : 2 * cols], preferred_element_type=jnp.float32)
    hidden = (gate / (1 + jnp.exp(-gate)) * up).astype(jnp.bfloat16)

    def share(slab):
        down = low_ref[pl.ds(pl.multiple_of(slab * width, width), width), 2 * cols :]
        return lax.dot_general(hidden, down, (((1,), (1,)), ((), ())), preferred_element_type=jnp.float32)

    for k in range(slabs // 2):
        other_ref[k] = share(2 * k + 1 - core[0]).astype(jnp.bfloat16)
        mine_ref[k] = share(2 * k + core[0])
    keep.wait()


def pair_kernel(mine_ref, got_ref, out_ref):
    out_ref[...] = (mine_ref[...] + got_ref[...].astype(jnp.float32)).astype(jnp.bfloat16)


def turn_kernel(low_ref, gate_ref, up_ref, down_ref):
    cols = gate_ref.shape[0]
    for k, ref in enumerate((gate_ref, up_ref, down_ref)):
        ref[...] = low_ref[:, k * cols : (k + 1) * cols].T


def sum_kernel(parts_ref, out_ref):
    total = parts_ref[0].astype(jnp.float32)
    for k in range(1, parts_ref.shape[0]):
        total += parts_ref[k].astype(jnp.float32)
    out_ref[...] = total.astype(jnp.bfloat16)


def device(z, y, t, tp):
    return (z * SIDE + y) * tp + t


def lines(tp, even, odd):
    groups = []
    for t in range(tp):
        for o in range(SIDE):
            along = (odd if t % 2 else even) == "y"
            groups.append([device(o, i, t, tp) if along else device(i, o, t, tp) for i in range(SIDE)])
    return groups


def on_device(prompt, norm_gain, gate_master, up_master, down_master):
    tp, fs = lax.axis_size("tp"), lax.axis_size("fs")
    tokens, width = prompt.shape
    rows, cols = gate_master.shape
    every = ("fs", "tp")
    gain_col = norm_gain[:, None]
    parts = [gate_master * gain_col, up_master * gain_col, down_master]
    sent = jnp.concatenate([(lax.reduce_precision(p, 8, 7) * SCALE).astype(jnp.float16) for p in parts], axis=1)
    whole = lax.all_to_all(jnp.broadcast_to(prompt, (tp, *prompt.shape)), "tp", 0, 0, tiled=True)
    own = lax.all_to_all(
        jnp.broadcast_to(sent, (SIDE, *sent.shape)), every, 0, 0, tiled=True, axis_index_groups=lines(tp, "y", "z")
    )
    filled = lax.all_gather(own.reshape(SIDE * rows, 3 * cols), every, axis=0, tiled=True, axis_index_groups=lines(tp, "z", "y"))
    near = (filled.astype(jnp.float32) * (1 / SCALE)).astype(jnp.bfloat16)
    core = (lax.axis_index("tp") % 2).astype(jnp.int32)[None]
    full = (rows * fs, 3 * cols)
    block = (tp // 2, tokens, width)
    other, mine, low = pl.pallas_call(
        hidden_kernel,
        out_shape=(struct(block), struct(block, jnp.float32), struct(full)),
        in_specs=[SMEM, VMEM, FAR],
        out_specs=(VMEM, VMEM, FAR),
        scratch_shapes=[
            pltpu.VMEM(full, jnp.bfloat16),
            pltpu.VMEM((tokens, tp * width), jnp.bfloat16),
            pltpu.SemaphoreType.DMA((SIDE, SIDE)),
            pltpu.SemaphoreType.DMA,
        ],
        compiler_params=pltpu.CompilerParams(vmem_limit_bytes=50 << 20),
    )(core, whole, near)
    got = lax.ppermute(other, "tp", [(t, t ^ 1) for t in range(tp)])
    paired = pl.pallas_call(
        pair_kernel,
        out_shape=struct(block),
        in_specs=[VMEM, VMEM],
        out_specs=VMEM,
        compiler_params=pltpu.CompilerParams(vmem_limit_bytes=8 << 20),
    )(mine, got)
    chips = [[t for t in range(c, tp, 2)] for c in range(2)]
    summed = lax.all_to_all(paired, "tp", 0, 0, tiled=True, axis_index_groups=chips)
    turned = struct((cols, rows * fs))
    gate_new, up_new, down_new = pl.pallas_call(
        turn_kernel,
        out_shape=(turned, turned, turned),
        grid=(rows * fs // width,),
        in_specs=[pl.BlockSpec((width, 3 * cols), lambda s: (s, 0))],
        out_specs=[pl.BlockSpec((cols, width), lambda s: (0, s))] * 3,
        compiler_params=pltpu.CompilerParams(vmem_limit_bytes=58 << 20),
        cost_estimate=pl.CostEstimate(flops=2 * 10**9, bytes_accessed=12 * rows * fs * cols, transcendentals=0),
    )(low)
    mixed = pl.pallas_call(
        sum_kernel,
        out_shape=struct((tokens, width)),
        in_specs=[VMEM],
        out_specs=VMEM,
        compiler_params=pltpu.CompilerParams(vmem_limit_bytes=6 << 20),
    )(summed)
    return gate_new, up_new, down_new, mixed.T


def solution(mesh):
    placed = (P("fs", "tp"), P("fs"), P("fs", "tp"), P("fs", "tp"), P("fs", "tp"))
    return jax.shard_map(
        on_device,
        mesh=mesh,
        in_specs=placed,
        out_specs=(P("tp", None), P("tp", None), P("tp", None), P("tp", "fs")),
        check_vma=False,
    )
```

time: 113 us -> 99.6 us (0.88)
  blocking collectives: 49 us -> 29.4 us
  Pallas kernels: 0 us -> 14 us
  local copies, waits for them, and re-layouts: 16.8 us -> 2.92 us
  waiting for transfers between devices: 8.07 us -> 18 us
  matrix products: 6.86 us -> 0 us
  starting transfers between devices: 24.9 us -> 29.8 us
  other arithmetic: 6.11 us -> 4.23 us
    all_gather x1, blocking collectives: 49 us -> 29.4 us  [on_device(): lax.all_gather(own.reshape(SIDE * rows, 3 * cols), every, axis=0, tiled=T...]
    pallas_call x0 -> x4, Pallas kernels: none -> 14 us  [the longest x1 7.03 us: on_device(): pl.pallas_call(turn_kernel, out_shape=(turned, turned, turned), grid=(row...]
    ppermute x0 -> x1, starting transfers between devices: none -> 10.2 us  [on_device(): got = lax.ppermute(other, 'tp', [(t, t ^ 1) for t in range(tp)])]
    all_to_all x2 -> x3, waiting for transfers between devices: 8.07 us -> 16.3 us  [the longest x1 13 us: on_device(): lax.all_to_all(jnp.broadcast_to(sent, (SIDE, *sent.shape)), every, 0, 0,...]
    unnamed x15 -> x0, local copies, waits for them, and re-layouts: 7.84 us -> none
    dot_general x2 -> x0, matrix products: 6.86 us -> none  [the longest x1 4.58 us: on_device(): lax.dot_general(down_w, hidden, (((1,), (1,)), ((), ())), preferred_eleme...]
    all_to_all x2 -> x3, starting transfers between devices: 24.9 us -> 19.6 us  [the longest x1 10.9 us: on_device(): lax.all_to_all(jnp.broadcast_to(sent, (SIDE, *sent.shape)), every, 0, 0,...]
    transpose x1 -> x0, local copies, waits for them, and re-layouts: 4 us -> none  [on_device(): return (gate_w.T, up_w.T, down_w.T, mixed)]
  transfers between devices with their start and end apart: 2 -> 4, of which waited for: 1 -> 3; matrix products, arithmetic and copies ran while one was open for 12% -> 3% of each run, Pallas kernels for 0% -> 7%
where the time goes in v2:
time: 99.6 us; the launch traced here: 99 us
  starting transfers between devices  29.8 us (30%)
  blocking collectives  29.4 us (30%)
  waiting for transfers between devices  18 us (18%)
  Pallas kernels  14 us (14%)
  other arithmetic  4.23 us (4%)
  local copies, waits for them, and re-layouts  2.92 us (3%)
    all_gather x1, blocking collectives, on_device(): lax.all_gather(own.reshape(SIDE * rows, 3 * cols), every, axis=0, tiled=T...  29.4 us
    all_to_all x1, waiting for transfers between devices, on_device(): lax.all_to_all(jnp.broadcast_to(sent, (SIDE, *sent.shape)), every, 0, 0,...  13 us
    all_to_all x1, starting transfers between devices, on_device(): lax.all_to_all(jnp.broadcast_to(sent, (SIDE, *sent.shape)), every, 0, 0,...  10.9 us
    ppermute x1, starting transfers between devices, on_device(): got = lax.ppermute(other, 'tp', [(t, t ^ 1) for t in range(tp)])  10.2 us
    pallas_call x1, Pallas kernels, on_device(): pl.pallas_call(turn_kernel, out_shape=(turned, turned, turned), grid=(row...  7.03 us
    pallas_call x1, Pallas kernels, on_device(): pl.pallas_call(hidden_kernel, out_shape=(struct(block), struct(block, jnp...  5.27 us
    all_to_all x1, starting transfers between devices, on_device(): lax.all_to_all(paired, 'tp', 0, 0, tiled=True, axis_index_groups=chips)  4.52 us
    all_to_all x1, starting transfers between devices, on_device(): lax.all_to_all(jnp.broadcast_to(prompt, (tp, *prompt.shape)), 'tp', 0, 0,...  4.21 us
  transfers between devices with their start and end apart: 4, of which 3 were waited for; matrix products, arithmetic and copies ran while one was open for 3% of the time, Pallas kernels for 7%

profile of v2, /device:TPU:1, one launch (start us, length us, event | category | flops | bytes accessed | tf_op | source)
XLA Modules:
  0.0 99.0 jit_solution(5685533298140932141)
XLA Ops:
  0.6 0.9 multiply_convert_fusion.3
  1.6 0.9 broadcast_in_dim.12
  2.5 10.9 %all-to-all-start.1 = ((f16[8,32,1152]{2,1,0:T(8,128)(2,1)}), f16[8,32,1152]{2,1,0:T(8,128)(2,1)S(1)}, u32[]{:S(2)}, u32[]{:S(2)}) async-start(f16[8,32,1152]{2,1,0:T(8,128)(2,1)} %broadcast_in_dim.12), calls=%async_computation.1 | async-start | bytes 1179648 | tf_op jit(solution)/shard_map/all_to_all | solution.py:95
  13.3 13.0 %all-to-all-done.1 = f16[8,32,1152]{2,1,0:T(8,128)(2,1)S(1)} async-done(((f16[8,32,1152]{2,1,0:T(8,128)(2,1)}), f16[8,32,1152]{2,1,0:T(8,128)(2,1)S(1)}, u32[]{:S(2)}, u32[]{:S(2)}) %all-to-all-start.1) | async-done | bytes 589856 | tf_op jit(solution)/shard_map/all_to_all | solution.py:95
  26.4 2.1 %broadcast_in_dim.11 = bf16[8,320,256]{2,1,0:T(8,128)(2,1)} broadcast(bf16[320,256]{1,0:T(8,128)(2,1)} %param.5), dimensions={1,2} | broadcast | bytes 1474560 | tf_op jit(solution)/shard_map/broadcast_in_dim | solution.py:94
  28.4 4.2 %all-to-all-start = ((bf16[8,320,256]{2,1,0:T(8,128)(2,1)}), bf16[8,320,256]{2,1,0:T(8,128)(2,1)S(1)}, u32[]{:S(2)}, u32[]{:S(2)}) async-start(bf16[8,320,256]{2,1,0:T(8,128)(2,1)} %broadcast_in_dim.11), calls=%async_computation | async-start | bytes 2621440 | tf_op jit(solution)/shard_map/all_to_all | solution.py:94
  32.6 29.4 %all-gather.1 = f16[2048,1152]{1,0:T(8,128)(2,1)S(1)} all-gather(f16[256,1152]{1,0:T(8,128)(2,1)S(1)} %bitcast.3), channel_id=1, replica_groups={{0,64,128,192,256,320,384,448},{8,72,136,200,264,328,392,456},{16,80,14..., dimensions={0}, use_global_device_ids=true | all-gather | bytes 5308416 | tf_op jit(solution)/shard_map/all_gather | solution.py:98
  62.0 3.3 %multiply_convert_fusion.near_ref = bf16[2048,1152]{1,0:T(8,128)(2,1)} fusion(f16[2048,1152]{1,0:T(8,128)(2,1)S(1)} %all-gather.1), kind=kLoop, calls=%fused_computation | loop fusion | flops 7077888 | bytes 9437184 | tf_op jit(solution)/shard_map/convert_element_type | solution.py:99
  65.3 0.0 all-to-all-done.x_ref
  65.3 5.3 %shard_map.84 = (bf16[4,320,256]{2,1,0:T(8,128)(2,1)S(1)}, f32[4,320,256]{2,1,0:T(8,128)S(1)}, bf16[2048,1152]{1,0:T(8,128)(2,1)}) custom-call(s32[1]{0:T(128)} %bitcast.core, bf16[8,320,256]{2,1,0:T(8,128)(2,1)S(1)} %all-to-all-done.x_ref, bf16[2048,1152]{1,0:T(8,128)(2,1)} %multiply_convert_fusion.near_ref), custom_call_target="tpu_custom_call" | custom-call | tf_op jit(solution)/shard_map/pallas_call | solution.py:103
  70.5 10.2 %collective-permute-start = (bf16[4,320,256]{2,1,0:T(8,128)(2,1)S(1)}, bf16[4,320,256]{2,1,0:T(8,128)(2,1)S(1)}, u32[]{:S(2)}, u32[]{:S(2)}) collective-permute-start(bf16[4,320,256]{2,1,0:T(8,128)(2,1)S(1)} %get-tuple-element.15), channel_id=1, source_target_pairs={{0,1},{1,0},{2,3},{3,2},{4,5},{5,4},{6,7},{7,6},{8,9},{9,8},{10,11... | collective-permute-start | bytes 1966088 | tf_op jit(solution)/shard_map/ppermute | solution.py:116
  80.8 1.7 %collective-permute-done.got_ref = bf16[4,320,256]{2,1,0:T(8,128)(2,1)S(1)} collective-permute-done((bf16[4,320,256]{2,1,0:T(8,128)(2,1)S(1)}, bf16[4,320,256]{2,1,0:T(8,128)(2,1)S(1)}, u32[]{:S(2)}, u32[]{:S(2)}) %collective-permute-start) | collective-permute-done | bytes 655392 | tf_op jit(solution)/shard_map/ppermute | solution.py:116
  82.5 1.0 shard_map.86
  83.4 4.5 %all-to-all-start.2 = ((bf16[4,320,256]{2,1,0:T(8,128)(2,1)}), bf16[4,320,256]{2,1,0:T(8,128)(2,1)S(1)}, u32[]{:S(2)}, u32[]{:S(2)}) async-start(bf16[4,320,256]{2,1,0:T(8,128)(2,1)} %shard_map.86), calls=%async_computation.2 | async-start | bytes 1310720 | tf_op jit(solution)/shard_map/all_to_all | solution.py:125
  88.0 7.0 %shard_map.85 = (bf16[384,2048]{1,0:T(8,128)(2,1)}, bf16[384,2048]{1,0:T(8,128)(2,1)}, bf16[384,2048]{1,0:T(8,128)(2,1)}) custom-call(bf16[2048,1152]{1,0:T(8,128)(2,1)} %get-tuple-element.10.low_ref), custom_call_target="tpu_custom_call" | custom-call | flops 2000000000 | bytes 9437184 | tf_op jit(solution)/shard_map/pallas_call | solution.py:127
  95.0 3.3 %all-to-all-done.2.parts_ref = bf16[4,320,256]{2,1,0:T(8,128)(2,1)S(1)} async-done(((bf16[4,320,256]{2,1,0:T(8,128)(2,1)}), bf16[4,320,256]{2,1,0:T(8,128)(2,1)S(1)}, u32[]{:S(2)}, u32[]{:S(2)}) %all-to-all-start.2) | async-done | bytes 655392 | tf_op jit(solution)/shard_map/all_to_all | solution.py:125
  98.3 0.7 shard_map.87
  (1 shorter events, 0.0 us)
Async XLA Ops:
  2.5 23.9 %all-to-all-start.1 = ((f16[8,32,1152]{2,1,0:T(8,128)(2,1)}), f16[8,32,1152]{2,1,0:T(8,128)(2,1)S(1)}, u32[]{:S(2)}, u32[]{:S(2)}) async-start(f16[8,32,1152]{2,1,0:T(8,128)(2,1)} %broadcast_in_dim.12), calls=%async_computation.1 | async-start | bytes 1179648 | tf_op jit(solution)/shard_map/all_to_all | solution.py:95
  28.4 36.8 %all-to-all-start = ((bf16[8,320,256]{2,1,0:T(8,128)(2,1)}), bf16[8,320,256]{2,1,0:T(8,128)(2,1)S(1)}, u32[]{:S(2)}, u32[]{:S(2)}) async-start(bf16[8,320,256]{2,1,0:T(8,128)(2,1)} %broadcast_in_dim.11), calls=%async_computation | async-start | bytes 2621440 | tf_op jit(solution)/shard_map/all_to_all | solution.py:94
  70.5 11.9 %collective-permute-start = (bf16[4,320,256]{2,1,0:T(8,128)(2,1)S(1)}, bf16[4,320,256]{2,1,0:T(8,128)(2,1)S(1)}, u32[]{:S(2)}, u32[]{:S(2)}) collective-permute-start(bf16[4,320,256]{2,1,0:T(8,128)(2,1)S(1)} %get-tuple-element.15), channel_id=1, source_target_pairs={{0,1},{1,0},{2,3},{3,2},{4,5},{5,4},{6,7},{7,6},{8,9},{9,8},{10,11... | collective-permute-start | bytes 1966088 | tf_op jit(solution)/shard_map/ppermute | solution.py:116
  83.4 14.8 %all-to-all-start.2 = ((bf16[4,320,256]{2,1,0:T(8,128)(2,1)}), bf16[4,320,256]{2,1,0:T(8,128)(2,1)S(1)}, u32[]{:S(2)}, u32[]{:S(2)}) async-start(bf16[4,320,256]{2,1,0:T(8,128)(2,1)} %shard_map.86), calls=%async_computation.2 | async-start | bytes 1310720 | tf_op jit(solution)/shard_map/all_to_all | solution.py:125

commit v3 on v2

--- a/solution.py
+++ b/solution.py
@@ -4,6 +4,7 @@
 from jax.experimental import pallas as pl
 from jax.experimental.pallas import tpu as pltpu
 from jax.sharding import PartitionSpec as P
+
 
 SIDE = 8
 SCALE = 2.0**18
@@ -16,15 +17,19 @@
     return jax.ShapeDtypeStruct(shape, dtype)
 
 
-def hidden_kernel(core, x_ref, near_ref, other_ref, mine_ref, kept_ref, low_ref, normed_ref, sems, keep_sem):
+def strides(core):
+    return jnp.where(core == 0, 1, SIDE), jnp.where(core == 0, SIDE, 1)
+
+
+def hidden_kernel(core, x_ref, near_ref, other_ref, mine_ref, low_ref, normed_ref, sems):
     slabs, tokens, width = x_ref.shape
     cols = low_ref.shape[1] // 3
     rows = low_ref.shape[0] // (SIDE * SIDE)
-    outer, inner = jnp.where(core[0] == 0, SIDE, 1), jnp.where(core[0] == 0, 1, SIDE)
+    along_z, along_y = strides(core[0])
     copies = []
     for z in range(SIDE):
         for y in range(SIDE):
-            row = pl.multiple_of((z * outer + y * inner) * rows, rows)
+            row = pl.multiple_of((z * along_z + y * along_y) * rows, rows)
             to = low_ref.at[pl.ds((z * SIDE + y) * rows, rows)]
             copies.append(pltpu.make_async_copy(near_ref.at[pl.ds(row, rows)], to, sems.at[z, y]))
             copies[-1].start()
@@ -35,12 +40,13 @@
     inverse = lax.rsqrt(jnp.sum(squares, axis=1, keepdims=True) / (slabs * width) + 1e-06)
     for s in range(slabs):
         normed_ref[:, s * width : (s + 1) * width] = (x_ref[s].astype(jnp.float32) * inverse).astype(jnp.bfloat16)
-    for copy in copies:
-        copy.wait()
-    keep = pltpu.make_async_copy(low_ref, kept_ref, keep_sem)
-    keep.start()
-    gate = jnp.dot(normed_ref[...], low_ref[:, :cols], preferred_element_type=jnp.float32)
-    up = jnp.dot(normed_ref[...], low_ref[:, cols : 2 * cols], preferred_element_type=jnp.float32)
+    both, half = 0.0, slabs * width // 2
+    for part in range(2):
+        for copy in copies[part * SIDE * SIDE // 2 : (part + 1) * SIDE * SIDE // 2]:
+            copy.wait()
+        ks = slice(part * half, (part + 1) * half)
+        both += jnp.dot(normed_ref[:, ks], low_ref[ks, : 2 * cols], preferred_element_type=jnp.float32)
+    gate, up = both[:, :cols], both[:, cols:]
     hidden = (gate / (1 + jnp.exp(-gate)) * up).astype(jnp.bfloat16)
 
     def share(slab):
@@ -50,17 +56,18 @@
     for k in range(slabs // 2):
         other_ref[k] = share(2 * k + 1 - core[0]).astype(jnp.bfloat16)
         mine_ref[k] = share(2 * k + core[0])
-    keep.wait()
 
 
 def pair_kernel(mine_ref, got_ref, out_ref):
     out_ref[...] = (mine_ref[...] + got_ref[...].astype(jnp.float32)).astype(jnp.bfloat16)
 
 
-def turn_kernel(low_ref, gate_ref, up_ref, down_ref):
-    cols = gate_ref.shape[0]
-    for k, ref in enumerate((gate_ref, up_ref, down_ref)):
-        ref[...] = low_ref[:, k * cols : (k + 1) * cols].T
+def turn_kernel(core, *refs):
+    pieces, outs = refs[:SIDE], refs[SIDE:]
+    cols = outs[0].shape[0]
+    for k, out in enumerate(outs):
+        slab = jnp.concatenate([piece[:, k * cols : (k + 1) * cols] for piece in pieces], axis=0)
+        out[...] = slab.T
 
 
 def sum_kernel(parts_ref, out_ref):
@@ -91,25 +98,24 @@
     gain_col = norm_gain[:, None]
     parts = [gate_master * gain_col, up_master * gain_col, down_master]
     sent = jnp.concatenate([(lax.reduce_precision(p, 8, 7) * SCALE).astype(jnp.float16) for p in parts], axis=1)
-    whole = lax.all_to_all(jnp.broadcast_to(prompt, (tp, *prompt.shape)), "tp", 0, 0, tiled=True)
-    own = lax.all_to_all(
-        jnp.broadcast_to(sent, (SIDE, *sent.shape)), every, 0, 0, tiled=True, axis_index_groups=lines(tp, "y", "z")
-    )
-    filled = lax.all_gather(own.reshape(SIDE * rows, 3 * cols), every, axis=0, tiled=True, axis_index_groups=lines(tp, "z", "y"))
+    copies = jnp.broadcast_to(sent, (SIDE, *sent.shape))
+    own = lax.all_to_all(copies, every, 0, 0, tiled=True, axis_index_groups=lines(tp, "z", "y"))
+    prompts = jnp.broadcast_to(prompt, (tp, *prompt.shape))
+    whole = lax.all_to_all(prompts, "tp", 0, 0, tiled=True)
+    filled = lax.all_gather(own.reshape(SIDE * rows, 3 * cols), every, axis=0, tiled=True, axis_index_groups=lines(tp, "y", "z"))
     near = (filled.astype(jnp.float32) * (1 / SCALE)).astype(jnp.bfloat16)
     core = (lax.axis_index("tp") % 2).astype(jnp.int32)[None]
     full = (rows * fs, 3 * cols)
     block = (tp // 2, tokens, width)
-    other, mine, low = pl.pallas_call(
+    other, mine = pl.pallas_call(
         hidden_kernel,
-        out_shape=(struct(block), struct(block, jnp.float32), struct(full)),
+        out_shape=(struct(block), struct(block, jnp.float32)),
         in_specs=[SMEM, VMEM, FAR],
-        out_specs=(VMEM, VMEM, FAR),
+        out_specs=(VMEM, VMEM),
         scratch_shapes=[
             pltpu.VMEM(full, jnp.bfloat16),
             pltpu.VMEM((tokens, tp * width), jnp.bfloat16),
             pltpu.SemaphoreType.DMA((SIDE, SIDE)),
-            pltpu.SemaphoreType.DMA,
         ],
         compiler_params=pltpu.CompilerParams(vmem_limit_bytes=50 << 20),
     )(core, whole, near)
@@ -124,15 +130,26 @@
     chips = [[t for t in range(c, tp, 2)] for c in range(2)]
     summed = lax.all_to_all(paired, "tp", 0, 0, tiled=True, axis_index_groups=chips)
     turned = struct((cols, rows * fs))
+
+    def piece(y):
+        def index(z, core):
+            along_z, along_y = strides(core[0])
+            return z * along_z + y * along_y, 0
+
+        return pl.BlockSpec((rows, 3 * cols), index)
+
     gate_new, up_new, down_new = pl.pallas_call(
         turn_kernel,
         out_shape=(turned, turned, turned),
-        grid=(rows * fs // width,),
-        in_specs=[pl.BlockSpec((width, 3 * cols), lambda s: (s, 0))],
-        out_specs=[pl.BlockSpec((cols, width), lambda s: (0, s))] * 3,
+        grid_spec=pltpu.PrefetchScalarGridSpec(
+            num_scalar_prefetch=1,
+            grid=(SIDE,),
+            in_specs=[piece(y) for y in range(SIDE)],
+            out_specs=[pl.BlockSpec((cols, SIDE * rows), lambda z, core: (0, z))] * 3,
+        ),
         compiler_params=pltpu.CompilerParams(vmem_limit_bytes=58 << 20),
         cost_estimate=pl.CostEstimate(flops=2 * 10**9, bytes_accessed=12 * rows * fs * cols, transcendentals=0),
-    )(low)
+    )(core, *[near] * SIDE)
     mixed = pl.pallas_call(
         sum_kernel,
         out_shape=struct((tokens, width)),

time: 99.6 us -> 98.3 us (0.987)
  starting transfers between devices: 29.8 us -> 27.7 us
    ppermute x1, starting transfers between devices: 10.2 us -> 5.98 us  [on_device(): got = lax.ppermute(other, 'tp', [(t, t ^ 1) for t in range(tp)])]
    all_to_all x2, starting transfers between devices: 15.1 us -> 17.3 us  [the longest x1 9.61 us: on_device(): whole = lax.all_to_all(prompts, 'tp', 0, 0, tiled=True)]
  transfers between devices with their start and end apart: 4 -> 4, of which waited for: 3 -> 3; matrix products, arithmetic and copies ran while one was open for 3% -> 3% of each run, Pallas kernels for 7% -> 8%
where the time goes in v3:
time: 98.3 us; the launch traced here: 97.5 us
  blocking collectives  29.8 us (30%)
  starting transfers between devices  27.7 us (28%)
  waiting for transfers between devices  17.4 us (18%)
  Pallas kernels  14.8 us (15%)
  other arithmetic  4.18 us (4%)
  local copies, waits for them, and re-layouts  2.92 us (3%)
    all_gather x1, blocking collectives, on_device(): lax.all_gather(own.reshape(SIDE * rows, 3 * cols), every, axis=0, tiled=T...  29.8 us
    all_to_all x1, waiting for transfers between devices, on_device(): lax.all_to_all(copies, every, 0, 0, tiled=True, axis_index_groups=lines(t...  12.8 us
    all_to_all x1, starting transfers between devices, on_device(): whole = lax.all_to_all(prompts, 'tp', 0, 0, tiled=True)  9.61 us
    all_to_all x1, starting transfers between devices, on_device(): lax.all_to_all(copies, every, 0, 0, tiled=True, axis_index_groups=lines(t...  7.64 us
    pallas_call x1, Pallas kernels, on_device(): pl.pallas_call(turn_kernel, out_shape=(turned, turned, turned), grid_spec...  7.48 us
    ppermute x1, starting transfers between devices, on_device(): got = lax.ppermute(other, 'tp', [(t, t ^ 1) for t in range(tp)])  5.98 us
    pallas_call x1, Pallas kernels, on_device(): pl.pallas_call(hidden_kernel, out_shape=(struct(block), struct(block, jnp...  5.59 us
    all_to_all x1, starting transfers between devices, on_device(): lax.all_to_all(paired, 'tp', 0, 0, tiled=True, axis_index_groups=chips)  4.51 us
  transfers between devices with their start and end apart: 4, of which 3 were waited for; matrix products, arithmetic and copies ran while one was open for 3% of the time, Pallas kernels for 8%

profile of v3, /device:TPU:1, one launch (start us, length us, event | category | flops | bytes accessed | tf_op | source)
XLA Modules:
  0.0 97.5 jit_solution(5283602359885344320)
XLA Ops:
  0.6 0.9 multiply_convert_fusion.3
  1.6 0.9 broadcast_in_dim.11
  2.5 7.6 %all-to-all-start = ((f16[8,32,1152]{2,1,0:T(8,128)(2,1)}), f16[8,32,1152]{2,1,0:T(8,128)(2,1)S(1)}, u32[]{:S(2)}, u32[]{:S(2)}) async-start(f16[8,32,1152]{2,1,0:T(8,128)(2,1)} %broadcast_in_dim.11), calls=%async_computation | async-start | bytes 1179648 | tf_op jit(solution)/shard_map/all_to_all | solution.py:102
  10.1 12.8 %all-to-all-done = f16[8,32,1152]{2,1,0:T(8,128)(2,1)S(1)} async-done(((f16[8,32,1152]{2,1,0:T(8,128)(2,1)}), f16[8,32,1152]{2,1,0:T(8,128)(2,1)S(1)}, u32[]{:S(2)}, u32[]{:S(2)}) %all-to-all-start) | async-done | bytes 589856 | tf_op jit(solution)/shard_map/all_to_all | solution.py:102
  23.0 2.1 %broadcast_in_dim.12 = bf16[8,320,256]{2,1,0:T(8,128)(2,1)} broadcast(bf16[320,256]{1,0:T(8,128)(2,1)} %param.5), dimensions={1,2} | broadcast | bytes 1474560 | tf_op jit(solution)/shard_map/broadcast_in_dim | solution.py:103
  25.0 9.6 %all-to-all-start.1 = ((bf16[8,320,256]{2,1,0:T(8,128)(2,1)}), bf16[8,320,256]{2,1,0:T(8,128)(2,1)S(1)}, u32[]{:S(2)}, u32[]{:S(2)}) async-start(bf16[8,320,256]{2,1,0:T(8,128)(2,1)} %broadcast_in_dim.12), calls=%async_computation.1 | async-start | bytes 2621440 | tf_op jit(solution)/shard_map/all_to_all | solution.py:104
  34.6 29.8 %all-gather.1 = f16[2048,1152]{1,0:T(8,128)(2,1)S(1)} all-gather(f16[256,1152]{1,0:T(8,128)(2,1)S(1)} %bitcast.3), channel_id=1, replica_groups={{0,8,16,24,32,40,48,56},{64,72,80,88,96,104,112,120},{128,136,144,152,1..., dimensions={0}, use_global_device_ids=true | all-gather | bytes 5308416 | tf_op jit(solution)/shard_map/all_gather | solution.py:105
  64.4 3.2 %multiply_convert_fusion.refs_0_.refs_1_.refs_2_.refs_3_.refs_4_.refs_5_.refs_6_.refs_7_.near_ref = bf16[2048,1152]{1,0:T(8,128)(2,1)} fusion(f16[2048,1152]{1,0:T(8,128)(2,1)S(1)} %all-gather.1), kind=kLoop, calls=%fused_computation | loop fusion | flops 7077888 | bytes 9437184 | tf_op jit(solution)/shard_map/convert_element_type | solution.py:106
  67.6 0.0 all-to-all-done.1.x_ref
  67.6 5.6 %shard_map.85 = (bf16[4,320,256]{2,1,0:T(8,128)(2,1)S(1)}, f32[4,320,256]{2,1,0:T(8,128)S(1)}) custom-call(s32[1]{0:T(128)} %bitcast.core, bf16[8,320,256]{2,1,0:T(8,128)(2,1)S(1)} %all-to-all-done.1.x_ref, bf16[2048,1152]{1,0:T(8,128)(2,1)} %multiply_convert_fusion.refs_0_.refs_1_.refs_2_.refs_3_.refs_4_.refs_5_.refs_6_.refs_7_.near_ref), custom_call_target="tpu_custom_call" | custom-call | tf_op jit(solution)/shard_map/pallas_call | solution.py:110
  73.2 6.0 %collective-permute-start = (bf16[4,320,256]{2,1,0:T(8,128)(2,1)S(1)}, bf16[4,320,256]{2,1,0:T(8,128)(2,1)S(1)}, u32[]{:S(2)}, u32[]{:S(2)}) collective-permute-start(bf16[4,320,256]{2,1,0:T(8,128)(2,1)S(1)} %get-tuple-element.13), channel_id=1, source_target_pairs={{0,1},{1,0},{2,3},{3,2},{4,5},{5,4},{6,7},{7,6},{8,9},{9,8},{10,11... | collective-permute-start | bytes 1966088 | tf_op jit(solution)/shard_map/ppermute | solution.py:122
  79.2 1.7 %collective-permute-done.got_ref = bf16[4,320,256]{2,1,0:T(8,128)(2,1)S(1)} collective-permute-done((bf16[4,320,256]{2,1,0:T(8,128)(2,1)S(1)}, bf16[4,320,256]{2,1,0:T(8,128)(2,1)S(1)}, u32[]{:S(2)}, u32[]{:S(2)}) %collective-permute-start) | collective-permute-done | bytes 655392 | tf_op jit(solution)/shard_map/ppermute | solution.py:122
  80.9 1.0 %shard_map.86 = bf16[4,320,256]{2,1,0:T(8,128)(2,1)} custom-call(f32[4,320,256]{2,1,0:T(8,128)S(1)} %get-tuple-element.12.mine_ref, bf16[4,320,256]{2,1,0:T(8,128)(2,1)S(1)} %collective-permute-done.got_ref), custom_call_target="tpu_custom_call" | custom-call | tf_op jit(solution)/shard_map/pallas_call | solution.py:123
  81.9 4.5 %all-to-all-start.2 = ((bf16[4,320,256]{2,1,0:T(8,128)(2,1)}), bf16[4,320,256]{2,1,0:T(8,128)(2,1)S(1)}, u32[]{:S(2)}, u32[]{:S(2)}) async-start(bf16[4,320,256]{2,1,0:T(8,128)(2,1)} %shard_map.86), calls=%async_computation.2 | async-start | bytes 1310720 | tf_op jit(solution)/shard_map/all_to_all | solution.py:131
  86.4 7.5 %shard_map.84 = (bf16[384,2048]{1,0:T(8,128)(2,1)}, bf16[384,2048]{1,0:T(8,128)(2,1)}, bf16[384,2048]{1,0:T(8,128)(2,1)}) custom-call(s32[1]{0:T(128)} %bitcast.core, bf16[2048,1152]{1,0:T(8,128)(2,1)} %multiply_convert_fusion.refs_0_.refs_1_.refs_2_.refs_3_.refs_4_.refs_5_.refs_6_.refs_7_.near_ref, ...), custom_call_target="tpu_custom_call" | custom-call | flops 2000000000 | bytes 9437184 | tf_op jit(solution)/shard_map/pallas_call | solution.py:141
  93.9 2.8 %all-to-all-done.2.parts_ref = bf16[4,320,256]{2,1,0:T(8,128)(2,1)S(1)} async-done(((bf16[4,320,256]{2,1,0:T(8,128)(2,1)}), bf16[4,320,256]{2,1,0:T(8,128)(2,1)S(1)}, u32[]{:S(2)}, u32[]{:S(2)}) %all-to-all-start.2) | async-done | bytes 655392 | tf_op jit(solution)/shard_map/all_to_all | solution.py:131
  96.7 0.7 shard_map.87
  (1 shorter events, 0.0 us)
Async XLA Ops:
  2.5 20.5 %all-to-all-start = ((f16[8,32,1152]{2,1,0:T(8,128)(2,1)}), f16[8,32,1152]{2,1,0:T(8,128)(2,1)S(1)}, u32[]{:S(2)}, u32[]{:S(2)}) async-start(f16[8,32,1152]{2,1,0:T(8,128)(2,1)} %broadcast_in_dim.11), calls=%async_computation | async-start | bytes 1179648 | tf_op jit(solution)/shard_map/all_to_all | solution.py:102
  25.0 42.6 %all-to-all-start.1 = ((bf16[8,320,256]{2,1,0:T(8,128)(2,1)}), bf16[8,320,256]{2,1,0:T(8,128)(2,1)S(1)}, u32[]{:S(2)}, u32[]{:S(2)}) async-start(bf16[8,320,256]{2,1,0:T(8,128)(2,1)} %broadcast_in_dim.12), calls=%async_computation.1 | async-start | bytes 2621440 | tf_op jit(solution)/shard_map/all_to_all | solution.py:104
  73.2 7.7 %collective-permute-start = (bf16[4,320,256]{2,1,0:T(8,128)(2,1)S(1)}, bf16[4,320,256]{2,1,0:T(8,128)(2,1)S(1)}, u32[]{:S(2)}, u32[]{:S(2)}) collective-permute-start(bf16[4,320,256]{2,1,0:T(8,128)(2,1)S(1)} %get-tuple-element.13), channel_id=1, source_target_pairs={{0,1},{1,0},{2,3},{3,2},{4,5},{5,4},{6,7},{7,6},{8,9},{9,8},{10,11... | collective-permute-start | bytes 1966088 | tf_op jit(solution)/shard_map/ppermute | solution.py:122
  81.9 14.8 %all-to-all-start.2 = ((bf16[4,320,256]{2,1,0:T(8,128)(2,1)}), bf16[4,320,256]{2,1,0:T(8,128)(2,1)S(1)}, u32[]{:S(2)}, u32[]{:S(2)}) async-start(bf16[4,320,256]{2,1,0:T(8,128)(2,1)} %shard_map.86), calls=%async_computation.2 | async-start | bytes 1310720 | tf_op jit(solution)/shard_map/all_to_all | solution.py:131

commit v4 on v3

v4 whole, which is shorter than its diff:
```python
import jax
import jax.numpy as jnp
from jax import lax
from jax.experimental import pallas as pl
from jax.experimental.pallas import tpu as pltpu
from jax.sharding import PartitionSpec as P


SIDE = 8
SCALE = 2.0**18
VMEM = pl.BlockSpec(memory_space=pltpu.VMEM)
SMEM = pl.BlockSpec(memory_space=pltpu.SMEM)


def struct(shape, dtype=jnp.bfloat16):
    return jax.ShapeDtypeStruct(shape, dtype)


def strides(core):
    return jnp.where(core == 0, 1, SIDE), jnp.where(core == 0, SIDE, 1)


def hidden_kernel(me, *refs):
    pairs, (near_ref, other_ref, mine_ref, normed_ref) = refs[: len(refs) - 4], refs[len(refs) - 4 :]
    chips = len(pairs)
    _, tokens, width = pairs[0].shape
    cols = near_ref.shape[-1] // 3
    core = lax.rem(me[0], 2)
    along_z, along_y = strides(core)
    squares = jnp.zeros((tokens, width), jnp.float32)
    for pair in pairs:
        for k in range(2):
            x = pair[k].astype(jnp.float32)
            squares += x * x
    inverse = lax.rsqrt(jnp.sum(squares, axis=1, keepdims=True) / (2 * chips * width) + 1e-06)
    for step, pair in enumerate(pairs):
        chip = lax.rem(me[0] // 2 + chips - step, chips)
        for k in range(2):
            slab = 2 * chip + (core if k == 0 else 1 - core)
            normed_ref[slab] = (pair[k].astype(jnp.float32) * inverse).astype(jnp.bfloat16)

    def weights(slab, columns):
        return jnp.concatenate([near_ref[slab * along_z + y * along_y, :, columns] for y in range(SIDE)], axis=0)

    both = 0.0
    for z in range(SIDE):
        both += jnp.dot(normed_ref[z], weights(z, slice(0, 2 * cols)), preferred_element_type=jnp.float32)
    gate, up = both[:, :cols], both[:, cols:]
    hidden = (gate / (1 + jnp.exp(-gate)) * up).astype(jnp.bfloat16)

    def share(slab):
        down = weights(slab, slice(2 * cols, 3 * cols))
        return lax.dot_general(hidden, down, (((1,), (1,)), ((), ())), preferred_element_type=jnp.float32)

    for k in range(chips):
        other_ref[k] = share(2 * k + 1 - core).astype(jnp.bfloat16)
        mine_ref[k] = share(2 * k + core)


def pair_kernel(mine_ref, got_ref, out_ref):
    out_ref[...] = (mine_ref[...] + got_ref[...].astype(jnp.float32)).astype(jnp.bfloat16)


def turn_kernel(me, *refs):
    pieces, outs = refs[:SIDE], refs[SIDE:]
    cols = outs[0].shape[0]
    for k, out in enumerate(outs):
        slab = jnp.concatenate([piece[:, k * cols : (k + 1) * cols] for piece in pieces], axis=0)
        out[...] = slab.T


def sum_kernel(parts_ref, out_ref):
    total = parts_ref[0].astype(jnp.float32)
    for k in range(1, parts_ref.shape[0]):
        total += parts_ref[k].astype(jnp.float32)
    out_ref[...] = total.astype(jnp.bfloat16)


def device(z, y, t, tp):
    return (z * SIDE + y) * tp + t


def lines(tp, even, odd):
    groups = []
    for t in range(tp):
        for o in range(SIDE):
            along = (odd if t % 2 else even) == "y"
            groups.append([device(o, i, t, tp) if along else device(i, o, t, tp) for i in range(SIDE)])
    return groups


def on_device(prompt, norm_gain, gate_master, up_master, down_master):
    tp, fs = lax.axis_size("tp"), lax.axis_size("fs")
    tokens, width = prompt.shape
    rows, cols = gate_master.shape
    every = ("fs", "tp")
    gain_col = norm_gain[:, None]
    parts = [gate_master * gain_col, up_master * gain_col, down_master]
    sent = jnp.concatenate([(lax.reduce_precision(p, 8, 7) * SCALE).astype(jnp.float16) for p in parts], axis=1)
    copies = jnp.broadcast_to(sent, (SIDE, *sent.shape))
    own = lax.all_to_all(copies, every, 0, 0, tiled=True, axis_index_groups=lines(tp, "z", "y"))
    partner = lax.ppermute(prompt, "tp", [(t, t ^ 1) for t in range(tp)])
    pairs = [jnp.stack([prompt, partner])]
    for step in range(1, tp // 2):
        pairs.append(lax.ppermute(pairs[0], "tp", [(t, (t + 2 * step) % tp) for t in range(tp)]))
    filled = lax.all_gather(own.reshape(SIDE * rows, 3 * cols), every, axis=0, tiled=True, axis_index_groups=lines(tp, "y", "z"))
    near = (filled.astype(jnp.float32) * (1 / SCALE)).astype(jnp.bfloat16)
    me = lax.axis_index("tp").astype(jnp.int32)[None]
    block = (tp // 2, tokens, width)
    other, mine = pl.pallas_call(
        hidden_kernel,
        out_shape=(struct(block), struct(block, jnp.float32)),
        in_specs=[SMEM] + [VMEM] * (tp // 2 + 1),
        out_specs=(VMEM, VMEM),
        scratch_shapes=[pltpu.VMEM((tp, tokens, width), jnp.bfloat16)],
        compiler_params=pltpu.CompilerParams(vmem_limit_bytes=16 << 20),
    )(me, *pairs, near.reshape(SIDE * SIDE, rows, 3 * cols))
    got = lax.ppermute(other, "tp", [(t, t ^ 1) for t in range(tp)])
    paired = pl.pallas_call(
        pair_kernel,
        out_shape=struct(block),
        in_specs=[VMEM, VMEM],
        out_specs=VMEM,
        compiler_params=pltpu.CompilerParams(vmem_limit_bytes=8 << 20),
    )(mine, got)
    chips = [[t for t in range(c, tp, 2)] for c in range(2)]
    summed = lax.all_to_all(paired, "tp", 0, 0, tiled=True, axis_index_groups=chips)
    turned = struct((cols, rows * fs))

    def piece(y):
        def index(z, me):
            along_z, along_y = strides(lax.rem(me[0], 2))
            return z * along_z + y * along_y, 0

        return pl.BlockSpec((rows, 3 * cols), index)

    gate_new, up_new, down_new = pl.pallas_call(
        turn_kernel,
        out_shape=(turned, turned, turned),
        grid_spec=pltpu.PrefetchScalarGridSpec(
            num_scalar_prefetch=1,
            grid=(SIDE,),
            in_specs=[piece(y) for y in range(SIDE)],
            out_specs=[pl.BlockSpec((cols, SIDE * rows), lambda z, me: (0, z))] * 3,
        ),
        compiler_params=pltpu.CompilerParams(vmem_limit_bytes=58 << 20),
        cost_estimate=pl.CostEstimate(flops=2 * 10**9, bytes_accessed=12 * rows * fs * cols, transcendentals=0),
    )(me, *[near] * SIDE)
    mixed = pl.pallas_call(
        sum_kernel,
        out_shape=struct((tokens, width)),
        in_specs=[VMEM],
        out_specs=VMEM,
        compiler_params=pltpu.CompilerParams(vmem_limit_bytes=6 << 20),
    )(summed)
    return gate_new, up_new, down_new, mixed.T


def solution(mesh):
    placed = (P("fs", "tp"), P("fs"), P("fs", "tp"), P("fs", "tp"), P("fs", "tp"))
    return jax.shard_map(
        on_device,
        mesh=mesh,
        in_specs=placed,
        out_specs=(P("tp", None), P("tp", None), P("tp", None), P("tp", "fs")),
        check_vma=False,
    )
```

time: 98.3 us -> 90.6 us (0.922)
  waiting for transfers between devices: 17.4 us -> 6 us
  starting transfers between devices: 27.7 us -> 33.6 us
  Pallas kernels: 14.8 us -> 12.4 us
  blocking collectives: 29.8 us -> 31.1 us
  other arithmetic: 4.18 us -> 3 us
    ppermute x0 -> x4, starting transfers between devices: none -> 16.6 us  [the longest x3 10.5 us: on_device(): lax.ppermute(pairs[0], 'tp', [(t, (t + 2 * step) % tp) for t in range(tp)])]
    all_to_all x1, waiting for transfers between devices: 12.8 us -> 0.01 us  [on_device(): lax.all_to_all(copies, every, 0, 0, tiled=True, axis_index_groups=lines(t...]
    all_to_all x1 -> x0, starting transfers between devices: 9.61 us -> none  [on_device(): whole = lax.all_to_all(prompts, 'tp', 0, 0, tiled=True)]
    pallas_call x1, Pallas kernels: 5.59 us -> 3.13 us  [on_device(): pl.pallas_call(hidden_kernel, out_shape=(struct(block), struct(block, jnp...]
    convert_element_type x1, other arithmetic: 3.21 us -> 1.08 us  [on_device(): near = (filled.astype(jnp.float32) * (1 / SCALE)).astype(jnp.bfloat16)]
    unnamed x0 -> x2, local copies, waits for them, and re-layouts: none -> 2.13 us
    broadcast_in_dim x1 -> x0, local copies, waits for them, and re-layouts: 2.06 us -> none  [on_device(): prompts = jnp.broadcast_to(prompt, (tp, *prompt.shape))]
    all_gather x1, blocking collectives: 29.8 us -> 31.1 us  [on_device(): lax.all_gather(own.reshape(SIDE * rows, 3 * cols), every, axis=0, tiled=T...]
  transfers between devices with their start and end apart: 4 -> 7, of which waited for: 3 -> 3; matrix products, arithmetic and copies ran while one was open for 3% -> 2% of each run, Pallas kernels for 8% -> 8%
where the time goes in v4:
time: 90.6 us; the launch traced here: 89.8 us
  starting transfers between devices  33.6 us (37%)
  blocking collectives  31.1 us (34%)
  Pallas kernels  12.4 us (14%)
  waiting for transfers between devices  6 us (7%)
  other arithmetic  3 us (3%)
  local copies, waits for them, and re-layouts  2.99 us (3%)
    all_gather x1, blocking collectives, on_device(): lax.all_gather(own.reshape(SIDE * rows, 3 * cols), every, axis=0, tiled=T...  31.1 us
    ppermute x3, starting transfers between devices, on_device(): lax.ppermute(pairs[0], 'tp', [(t, (t + 2 * step) % tp) for t in range(tp)])  10.5 us
    all_to_all x1, starting transfers between devices, on_device(): lax.all_to_all(copies, every, 0, 0, tiled=True, axis_index_groups=lines(t...  7.64 us
    pallas_call x1, Pallas kernels, on_device(): pl.pallas_call(turn_kernel, out_shape=(turned, turned, turned), grid_spec...  7.5 us
    ppermute x1, starting transfers between devices, on_device(): partner = lax.ppermute(prompt, 'tp', [(t, t ^ 1) for t in range(tp)])  6.07 us
    ppermute x1, starting transfers between devices, on_device(): got = lax.ppermute(other, 'tp', [(t, t ^ 1) for t in range(tp)])  5.89 us
    all_to_all x1, starting transfers between devices, on_device(): lax.all_to_all(paired, 'tp', 0, 0, tiled=True, axis_index_groups=chips)  3.48 us
    pallas_call x1, Pallas kernels, on_device(): pl.pallas_call(hidden_kernel, out_shape=(struct(block), struct(block, jnp...  3.13 us
  transfers between devices with their start and end apart: 7, of which 3 were waited for; matrix products, arithmetic and copies ran while one was open for 2% of the time, Pallas kernels for 8%

profile of v4, /device:TPU:1, one launch (start us, length us, event | category | flops | bytes accessed | tf_op | source)
XLA Modules:
  0.0 89.8 jit_solution(15748115764960855897)
XLA Ops:
  0.6 0.9 %multiply_convert_fusion.3 = (f16[32,384]{1,0:T(8,128)(2,1)S(1)}, f16[32,384]{1,0:T(8,128)(2,1)S(1)}, f16[32,384]{1,0:T(8,128)(2,1)S(1)}) fusion(f32[32,384]{1,0:T(8,128)} %param.7, f32[32]{0:T(128)} %param.6, f32[32,384]{1,0:T(8,128)} %param.8, f32[32,384]{1,0:T(8,128)} %param.9), kind=kLoop, calls=%fused_computation.5 | loop fusion | flops 135168 | bytes 221312 | tf_op jit(solution)/shard_map/convert_element_type | solution.py:99
  1.6 0.9 broadcast_in_dim.8
  2.5 7.6 %all-to-all-start = ((f16[8,32,1152]{2,1,0:T(8,128)(2,1)}), f16[8,32,1152]{2,1,0:T(8,128)(2,1)S(1)}, u32[]{:S(2)}, u32[]{:S(2)}) async-start(f16[8,32,1152]{2,1,0:T(8,128)(2,1)} %broadcast_in_dim.8), calls=%async_computation | async-start | bytes 1179648 | tf_op jit(solution)/shard_map/all_to_all | solution.py:101
  10.1 6.1 %collective-permute-start = (bf16[320,256]{1,0:T(8,128)(2,1)}, bf16[320,256]{1,0:T(8,128)(2,1)S(1)}, u32[]{:S(2)}, u32[]{:S(2)}) collective-permute-start(bf16[320,256]{1,0:T(8,128)(2,1)} %param.5), channel_id=1, source_target_pairs={{0,1},{1,0},{2,3},{3,2},{4,5},{5,4},{6,7},{7,6},{8,9},{9,8},{10,11... | collective-permute-start | bytes 491528 | tf_op jit(solution)/shard_map/ppermute | solution.py:102
  16.2 1.2 %collective-permute-done = bf16[320,256]{1,0:T(8,128)(2,1)S(1)} collective-permute-done((bf16[320,256]{1,0:T(8,128)(2,1)}, bf16[320,256]{1,0:T(8,128)(2,1)S(1)}, u32[]{:S(2)}, u32[]{:S(2)}) %collective-permute-start) | collective-permute-done | bytes 163872 | tf_op jit(solution)/shard_map/ppermute | solution.py:102
  17.4 0.9 %pad_maximum_fusion.refs_0_ = bf16[2,320,256]{2,1,0:T(8,128)(2,1)S(1)} fusion(bf16[1,320,256]{2,1,0:T(8,128)(2,1)S(1)} %bitcast.9, bf16[1,320,256]{2,1,0:T(8,128)(2,1)} %bitcast.8), kind=kLoop, calls=%fused_computation.1 | loop fusion | flops 163840 | bytes 655360 | tf_op jit(solution)/shard_map/stack | solution.py:103
  18.4 3.1 %collective-permute-start.1 = (bf16[2,320,256]{2,1,0:T(8,128)(2,1)S(1)}, bf16[2,320,256]{2,1,0:T(8,128)(2,1)S(1)}, u32[]{:S(2)}, u32[]{:S(2)}) collective-permute-start(bf16[2,320,256]{2,1,0:T(8,128)(2,1)S(1)} %pad_maximum_fusion.refs_0_), channel_id=1, source_target_pairs={{0,2},{1,3},{2,4},{3,5},{4,6},{5,7},{6,0},{7,1},{8,10},{9,11},{10,... | collective-permute-start | bytes 983048 | tf_op jit(solution)/shard_map/ppermute | solution.py:105
  21.5 4.4 %collective-permute-start.2 = (bf16[2,320,256]{2,1,0:T(8,128)(2,1)S(1)}, bf16[2,320,256]{2,1,0:T(8,128)(2,1)S(1)}, u32[]{:S(2)}, u32[]{:S(2)}) collective-permute-start(bf16[2,320,256]{2,1,0:T(8,128)(2,1)S(1)} %pad_maximum_fusion.refs_0_), channel_id=1, source_target_pairs={{0,4},{1,5},{2,6},{3,7},{4,0},{5,1},{6,2},{7,3},{8,12},{9,13},{10,... | collective-permute-start | bytes 983048 | tf_op jit(solution)/shard_map/ppermute | solution.py:105
  25.9 3.1 %collective-permute-start.3 = (bf16[2,320,256]{2,1,0:T(8,128)(2,1)S(1)}, bf16[2,320,256]{2,1,0:T(8,128)(2,1)S(1)}, u32[]{:S(2)}, u32[]{:S(2)}) collective-permute-start(bf16[2,320,256]{2,1,0:T(8,128)(2,1)S(1)} %pad_maximum_fusion.refs_0_), channel_id=1, source_target_pairs={{0,6},{1,7},{2,0},{3,1},{4,2},{5,3},{6,4},{7,5},{8,14},{9,15},{10,... | collective-permute-start | bytes 983048 | tf_op jit(solution)/shard_map/ppermute | solution.py:105
  28.9 0.0 all-to-all-done
  28.9 31.1 %all-gather.1 = f16[2048,1152]{1,0:T(8,128)(2,1)S(1)} all-gather(f16[256,1152]{1,0:T(8,128)(2,1)S(1)} %bitcast.7), channel_id=1, replica_groups={{0,8,16,24,32,40,48,56},{64,72,80,88,96,104,112,120},{128,136,144,152,1..., dimensions={0}, use_global_device_ids=true | all-gather | bytes 5308416 | tf_op jit(solution)/shard_map/all_gather | solution.py:106
  60.0 1.1 %multiply_convert_fusion.refs_0_.refs_1_.refs_2_.refs_3_.refs_4_.refs_5_.refs_6_.refs_7_ = bf16[2048,1152]{1,0:T(8,128)(2,1)S(1)} fusion(f16[2048,1152]{1,0:T(8,128)(2,1)S(1)} %all-gather.1), kind=kLoop, calls=%fused_computation | loop fusion | flops 7077888 | bytes 9437184 | tf_op jit(solution)/shard_map/convert_element_type | solution.py:107
  61.1 0.0 collective-permute-done.1.refs_1_
  61.1 0.0 collective-permute-done.2.refs_2_
  61.1 0.0 collective-permute-done.3.refs_3_
  61.1 3.1 %shard_map.85 = (bf16[4,320,256]{2,1,0:T(8,128)(2,1)S(1)}, f32[4,320,256]{2,1,0:T(8,128)S(1)}) custom-call(s32[1]{0:T(128)} %bitcast.me, bf16[2,320,256]{2,1,0:T(8,128)(2,1)S(1)} %pad_maximum_fusion.refs_0_, bf16[2,320,256]{2,1,0:T(8,128)(2,1)S(1)} %collective-permute-done.1.refs_1_, bf16[2,320,256]{2,1,0:T(8,128)(2,1)S(1)} %collective-permute-done.2.refs_2_, ...), custom_call_target="tpu_custom_call" | custom-call | tf_op jit(solution)/shard_map/pallas_call | solution.py:110
  64.3 2.1 %copy-done = bf16[2048,1152]{1,0:T(8,128)(2,1)} copy-done((bf16[2048,1152]{1,0:T(8,128)(2,1)}, bf16[2048,1152]{1,0:T(8,128)(2,1)S(1)}, u32[]{:S(2)}) %copy-start) | copy-done | bytes 4718616
  66.4 5.9 %collective-permute-start.4 = (bf16[4,320,256]{2,1,0:T(8,128)(2,1)S(1)}, bf16[4,320,256]{2,1,0:T(8,128)(2,1)S(1)}, u32[]{:S(2)}, u32[]{:S(2)}) collective-permute-start(bf16[4,320,256]{2,1,0:T(8,128)(2,1)S(1)} %get-tuple-element.13), channel_id=1, source_target_pairs={{0,1},{1,0},{2,3},{3,2},{4,5},{5,4},{6,7},{7,6},{8,9},{9,8},{10,11... | collective-permute-start | bytes 1966088 | tf_op jit(solution)/shard_map/ppermute | solution.py:118
  72.3 1.7 %collective-permute-done.4.got_ref = bf16[4,320,256]{2,1,0:T(8,128)(2,1)S(1)} collective-permute-done((bf16[4,320,256]{2,1,0:T(8,128)(2,1)S(1)}, bf16[4,320,256]{2,1,0:T(8,128)(2,1)S(1)}, u32[]{:S(2)}, u32[]{:S(2)}) %collective-permute-start.4) | collective-permute-done | bytes 655392 | tf_op jit(solution)/shard_map/ppermute | solution.py:118
  74.0 1.0 %shard_map.86 = bf16[4,320,256]{2,1,0:T(8,128)(2,1)} custom-call(f32[4,320,256]{2,1,0:T(8,128)S(1)} %get-tuple-element.12.mine_ref, bf16[4,320,256]{2,1,0:T(8,128)(2,1)S(1)} %collective-permute-done.4.got_ref), custom_call_target="tpu_custom_call" | custom-call | tf_op jit(solution)/shard_map/pallas_call | solution.py:119
  75.0 3.5 %all-to-all-start.1 = ((bf16[4,320,256]{2,1,0:T(8,128)(2,1)}), bf16[4,320,256]{2,1,0:T(8,128)(2,1)S(1)}, u32[]{:S(2)}, u32[]{:S(2)}) async-start(bf16[4,320,256]{2,1,0:T(8,128)(2,1)} %shard_map.86), calls=%async_computation.1 | async-start | bytes 1310720 | tf_op jit(solution)/shard_map/all_to_all | solution.py:127
  78.5 7.5 %shard_map.84 = (bf16[384,2048]{1,0:T(8,128)(2,1)}, bf16[384,2048]{1,0:T(8,128)(2,1)}, bf16[384,2048]{1,0:T(8,128)(2,1)}) custom-call(s32[1]{0:T(128)} %bitcast.me, bf16[2048,1152]{1,0:T(8,128)(2,1)} %copy-done, bf16[2048,1152]{1,0:T(8,128)(2,1)} %copy-done, bf16[2048,1152]{1,0:T(8,128)(2,1)} %copy-done, bf16[2048,1152]{1,0:T(8,128)(2,1)} %copy-done, ...), custom_call_target="tpu_custom_call" | custom-call | flops 2000000000 | bytes 9437184 | tf_op jit(solution)/shard_map/pallas_call | solution.py:137
  86.0 3.1 %all-to-all-done.1.parts_ref = bf16[4,320,256]{2,1,0:T(8,128)(2,1)S(1)} async-done(((bf16[4,320,256]{2,1,0:T(8,128)(2,1)}), bf16[4,320,256]{2,1,0:T(8,128)(2,1)S(1)}, u32[]{:S(2)}, u32[]{:S(2)}) %all-to-all-start.1) | async-done | bytes 655392 | tf_op jit(solution)/shard_map/all_to_all | solution.py:127
  89.0 0.7 shard_map.87
  (2 shorter events, 0.0 us)
Async XLA Ops:
  2.5 26.4 %all-to-all-start = ((f16[8,32,1152]{2,1,0:T(8,128)(2,1)}), f16[8,32,1152]{2,1,0:T(8,128)(2,1)S(1)}, u32[]{:S(2)}, u32[]{:S(2)}) async-start(f16[8,32,1152]{2,1,0:T(8,128)(2,1)} %broadcast_in_dim.8), calls=%async_computation | async-start | bytes 1179648 | tf_op jit(solution)/shard_map/all_to_all | solution.py:101
  10.1 7.3 %collective-permute-start = (bf16[320,256]{1,0:T(8,128)(2,1)}, bf16[320,256]{1,0:T(8,128)(2,1)S(1)}, u32[]{:S(2)}, u32[]{:S(2)}) collective-permute-start(bf16[320,256]{1,0:T(8,128)(2,1)} %param.5), channel_id=1, source_target_pairs={{0,1},{1,0},{2,3},{3,2},{4,5},{5,4},{6,7},{7,6},{8,9},{9,8},{10,11... | collective-permute-start | bytes 491528 | tf_op jit(solution)/shard_map/ppermute | solution.py:102
  18.4 42.7 %collective-permute-start.1 = (bf16[2,320,256]{2,1,0:T(8,128)(2,1)S(1)}, bf16[2,320,256]{2,1,0:T(8,128)(2,1)S(1)}, u32[]{:S(2)}, u32[]{:S(2)}) collective-permute-start(bf16[2,320,256]{2,1,0:T(8,128)(2,1)S(1)} %pad_maximum_fusion.refs_0_), channel_id=1, source_target_pairs={{0,2},{1,3},{2,4},{3,5},{4,6},{5,7},{6,0},{7,1},{8,10},{9,11},{10,... | collective-permute-start | bytes 983048 | tf_op jit(solution)/shard_map/ppermute | solution.py:105
  21.5 39.6 %collective-permute-start.2 = (bf16[2,320,256]{2,1,0:T(8,128)(2,1)S(1)}, bf16[2,320,256]{2,1,0:T(8,128)(2,1)S(1)}, u32[]{:S(2)}, u32[]{:S(2)}) collective-permute-start(bf16[2,320,256]{2,1,0:T(8,128)(2,1)S(1)} %pad_maximum_fusion.refs_0_), channel_id=1, source_target_pairs={{0,4},{1,5},{2,6},{3,7},{4,0},{5,1},{6,2},{7,3},{8,12},{9,13},{10,... | collective-permute-start | bytes 983048 | tf_op jit(solution)/shard_map/ppermute | solution.py:105
  25.9 35.2 %collective-permute-start.3 = (bf16[2,320,256]{2,1,0:T(8,128)(2,1)S(1)}, bf16[2,320,256]{2,1,0:T(8,128)(2,1)S(1)}, u32[]{:S(2)}, u32[]{:S(2)}) collective-permute-start(bf16[2,320,256]{2,1,0:T(8,128)(2,1)S(1)} %pad_maximum_fusion.refs_0_), channel_id=1, source_target_pairs={{0,6},{1,7},{2,0},{3,1},{4,2},{5,3},{6,4},{7,5},{8,14},{9,15},{10,... | collective-permute-start | bytes 983048 | tf_op jit(solution)/shard_map/ppermute | solution.py:105
  64.2 2.1 %copy-start = (bf16[2048,1152]{1,0:T(8,128)(2,1)}, bf16[2048,1152]{1,0:T(8,128)(2,1)S(1)}, u32[]{:S(2)}) copy-start(bf16[2048,1152]{1,0:T(8,128)(2,1)S(1)} %multiply_convert_fusion.refs_0_.refs_1_.refs_2_.refs_3_.refs_4_.refs_5_.refs_6_.refs_7_) | copy-start | bytes 14155780
  66.4 7.6 %collective-permute-start.4 = (bf16[4,320,256]{2,1,0:T(8,128)(2,1)S(1)}, bf16[4,320,256]{2,1,0:T(8,128)(2,1)S(1)}, u32[]{:S(2)}, u32[]{:S(2)}) collective-permute-start(bf16[4,320,256]{2,1,0:T(8,128)(2,1)S(1)} %get-tuple-element.13), channel_id=1, source_target_pairs={{0,1},{1,0},{2,3},{3,2},{4,5},{5,4},{6,7},{7,6},{8,9},{9,8},{10,11... | collective-permute-start | bytes 1966088 | tf_op jit(solution)/shard_map/ppermute | solution.py:118
  75.0 14.1 %all-to-all-start.1 = ((bf16[4,320,256]{2,1,0:T(8,128)(2,1)}), bf16[4,320,256]{2,1,0:T(8,128)(2,1)S(1)}, u32[]{:S(2)}, u32[]{:S(2)}) async-start(bf16[4,320,256]{2,1,0:T(8,128)(2,1)} %shard_map.86), calls=%async_computation.1 | async-start | bytes 1310720 | tf_op jit(solution)/shard_map/all_to_all | solution.py:127

commit v5 on v4

--- a/solution.py
+++ b/solution.py
@@ -20,32 +20,37 @@
     return jnp.where(core == 0, 1, SIDE), jnp.where(core == 0, SIDE, 1)
 
 
+def lift_kernel(prompt_ref, out_ref):
+    out_ref[...] = prompt_ref[...]
+
+
+def stack_kernel(first_ref, second_ref, out_ref):
+    out_ref[0] = first_ref[...]
+    out_ref[1] = second_ref[...]
+
+
 def hidden_kernel(me, *refs):
-    pairs, (near_ref, other_ref, mine_ref, normed_ref) = refs[: len(refs) - 4], refs[len(refs) - 4 :]
+    pairs, (near_ref, other_ref, mine_ref) = refs[: len(refs) - 3], refs[len(refs) - 3 :]
     chips = len(pairs)
     _, tokens, width = pairs[0].shape
     cols = near_ref.shape[-1] // 3
     core = lax.rem(me[0], 2)
     along_z, along_y = strides(core)
-    squares = jnp.zeros((tokens, width), jnp.float32)
-    for pair in pairs:
-        for k in range(2):
-            x = pair[k].astype(jnp.float32)
-            squares += x * x
-    inverse = lax.rsqrt(jnp.sum(squares, axis=1, keepdims=True) / (2 * chips * width) + 1e-06)
+
+    def weights(slab, columns):
+        at = [slab * along_z + y * along_y for y in range(SIDE)]
+        return jnp.concatenate([near_ref[row, :, columns] for row in at], axis=0)
+
+    squares, both = jnp.zeros((tokens, width), jnp.float32), 0.0
     for step, pair in enumerate(pairs):
         chip = lax.rem(me[0] // 2 + chips - step, chips)
         for k in range(2):
+            x = pair[k]
             slab = 2 * chip + (core if k == 0 else 1 - core)
-            normed_ref[slab] = (pair[k].astype(jnp.float32) * inverse).astype(jnp.bfloat16)
-
-    def weights(slab, columns):
-        return jnp.concatenate([near_ref[slab * along_z + y * along_y, :, columns] for y in range(SIDE)], axis=0)
-
-    both = 0.0
-    for z in range(SIDE):
-        both += jnp.dot(normed_ref[z], weights(z, slice(0, 2 * cols)), preferred_element_type=jnp.float32)
-    gate, up = both[:, :cols], both[:, cols:]
+            both += jnp.dot(x, weights(slab, slice(0, 2 * cols)), preferred_element_type=jnp.float32)
+            squares += x.astype(jnp.float32) * x.astype(jnp.float32)
+    inverse = lax.rsqrt(jnp.sum(squares, axis=1, keepdims=True) / (2 * chips * width) + 1e-06)
+    gate, up = both[:, :cols] * inverse, both[:, cols:] * inverse
     hidden = (gate / (1 + jnp.exp(-gate)) * up).astype(jnp.bfloat16)
 
     def share(slab):
@@ -61,11 +66,12 @@
     out_ref[...] = (mine_ref[...] + got_ref[...].astype(jnp.float32)).astype(jnp.bfloat16)
 
 
-def turn_kernel(me, *refs):
-    pieces, outs = refs[:SIDE], refs[SIDE:]
+def turn_kernel(me, near_ref, *outs):
     cols = outs[0].shape[0]
+    along_z, along_y = strides(lax.rem(me[0], 2))
+    at = [pl.program_id(0) * along_z + y * along_y for y in range(SIDE)]
     for k, out in enumerate(outs):
-        slab = jnp.concatenate([piece[:, k * cols : (k + 1) * cols] for piece in pieces], axis=0)
+        slab = jnp.concatenate([near_ref[row, :, k * cols : (k + 1) * cols] for row in at], axis=0)
         out[...] = slab.T
 
 
@@ -100,7 +106,22 @@
     copies = jnp.broadcast_to(sent, (SIDE, *sent.shape))
     own = lax.all_to_all(copies, every, 0, 0, tiled=True, axis_index_groups=lines(tp, "z", "y"))
     partner = lax.ppermute(prompt, "tp", [(t, t ^ 1) for t in range(tp)])
-    pairs = [jnp.stack([prompt, partner])]
+    own_prompt = pl.pallas_call(
+        lift_kernel,
+        out_shape=struct((tokens, width)),
+        in_specs=[VMEM],
+        out_specs=VMEM,
+        compiler_params=pltpu.CompilerParams(vmem_limit_bytes=4 << 20),
+    )(prompt)
+    pairs = [
+        pl.pallas_call(
+            stack_kernel,
+            out_shape=struct((2, tokens, width)),
+            in_specs=[VMEM, VMEM],
+            out_specs=VMEM,
+            compiler_params=pltpu.CompilerParams(vmem_limit_bytes=4 << 20),
+        )(own_prompt, partner)
+    ]
     for step in range(1, tp // 2):
         pairs.append(lax.ppermute(pairs[0], "tp", [(t, (t + 2 * step) % tp) for t in range(tp)]))
     filled = lax.all_gather(own.reshape(SIDE * rows, 3 * cols), every, axis=0, tiled=True, axis_index_groups=lines(tp, "y", "z"))
@@ -112,7 +133,6 @@
         out_shape=(struct(block), struct(block, jnp.float32)),
         in_specs=[SMEM] + [VMEM] * (tp // 2 + 1),
         out_specs=(VMEM, VMEM),
-        scratch_shapes=[pltpu.VMEM((tp, tokens, width), jnp.bfloat16)],
         compiler_params=pltpu.CompilerParams(vmem_limit_bytes=16 << 20),
     )(me, *pairs, near.reshape(SIDE * SIDE, rows, 3 * cols))
     got = lax.ppermute(other, "tp", [(t, t ^ 1) for t in range(tp)])
@@ -127,25 +147,18 @@
     summed = lax.all_to_all(paired, "tp", 0, 0, tiled=True, axis_index_groups=chips)
     turned = struct((cols, rows * fs))
 
-    def piece(y):
-        def index(z, me):
-            along_z, along_y = strides(lax.rem(me[0], 2))
-            return z * along_z + y * along_y, 0
-
-        return pl.BlockSpec((rows, 3 * cols), index)
-
     gate_new, up_new, down_new = pl.pallas_call(
         turn_kernel,
         out_shape=(turned, turned, turned),
         grid_spec=pltpu.PrefetchScalarGridSpec(
             num_scalar_prefetch=1,
             grid=(SIDE,),
-            in_specs=[piece(y) for y in range(SIDE)],
+            in_specs=[VMEM],
             out_specs=[pl.BlockSpec((cols, SIDE * rows), lambda z, me: (0, z))] * 3,
         ),
-        compiler_params=pltpu.CompilerParams(vmem_limit_bytes=58 << 20),
+        compiler_params=pltpu.CompilerParams(vmem_limit_bytes=16 << 20),
         cost_estimate=pl.CostEstimate(flops=2 * 10**9, bytes_accessed=12 * rows * fs * cols, transcendentals=0),
-    )(me, *[near] * SIDE)
+    )(me, near.reshape(SIDE * SIDE, rows, 3 * cols))
     mixed = pl.pallas_call(
         sum_kernel,
         out_shape=struct((tokens, width)),

time: 90.6 us -> 88.9 us (0.981)
  Pallas kernels: 12.4 us -> 8.38 us
  local copies, waits for them, and re-layouts: 2.99 us -> 6.22 us
  other arithmetic: 3 us -> 2.05 us
    pallas_call x1, Pallas kernels: 7.5 us -> 3.95 us  [on_device(): pl.pallas_call(turn_kernel, out_shape=(turned, turned, turned), grid_spec...]
    unnamed x2 -> x6, local copies, waits for them, and re-layouts: 2.13 us -> 5.36 us
    all_to_all x1, waiting for transfers between devices: 3.07 us -> 4.28 us  [on_device(): lax.all_to_all(paired, 'tp', 0, 0, tiled=True, axis_index_groups=chips)]
    another operation x1 -> x0, other arithmetic: 0.95 us -> none  [on_device(): pairs = [jnp.stack([prompt, partner])]]
    ppermute x1, waiting for transfers between devices: 1.21 us -> 0.28 us  [on_device(): partner = lax.ppermute(prompt, 'tp', [(t, t ^ 1) for t in range(tp)])]
  transfers between devices with their start and end apart: 7 -> 7, of which waited for: 3 -> 3; matrix products, arithmetic and copies ran while one was open for 2% -> 1% of each run, Pallas kernels for 8% -> 5%
where the time goes in v5:
time: 88.9 us; the launch traced here: 88.4 us
  starting transfers between devices  33.6 us (38%)
  blocking collectives  31.1 us (35%)
  Pallas kernels  8.38 us (9%)
  waiting for transfers between devices  6.27 us (7%)
  local copies, waits for them, and re-layouts  6.22 us (7%)
  other arithmetic  2.05 us (2%)
    all_gather x1, blocking collectives, on_device(): lax.all_gather(own.reshape(SIDE * rows, 3 * cols), every, axis=0, tiled=T...  31.1 us
    ppermute x3, starting transfers between devices, on_device(): lax.ppermute(pairs[0], 'tp', [(t, (t + 2 * step) % tp) for t in range(tp)])  10.5 us
    all_to_all x1, starting transfers between devices, on_device(): lax.all_to_all(copies, every, 0, 0, tiled=True, axis_index_groups=lines(t...  7.64 us
    ppermute x1, starting transfers between devices, on_device(): partner = lax.ppermute(prompt, 'tp', [(t, t ^ 1) for t in range(tp)])  6.07 us
    ppermute x1, starting transfers between devices, on_device(): got = lax.ppermute(other, 'tp', [(t, t ^ 1) for t in range(tp)])  5.87 us
    unnamed x6, local copies, waits for them, and re-layouts  5.36 us
    all_to_all x1, waiting for transfers between devices, on_device(): lax.all_to_all(paired, 'tp', 0, 0, tiled=True, axis_index_groups=chips)  4.28 us
    pallas_call x1, Pallas kernels, on_device(): pl.pallas_call(turn_kernel, out_shape=(turned, turned, turned), grid_spec...  3.95 us
  transfers between devices with their start and end apart: 7, of which 3 were waited for; matrix products, arithmetic and copies ran while one was open for 1% of the time, Pallas kernels for 5%

profile of v5, /device:TPU:1, one launch (start us, length us, event | category | flops | bytes accessed | tf_op | source)
XLA Modules:
  0.0 88.4 jit_solution(12689535818819984245)
XLA Ops:
  0.6 0.9 %multiply_convert_fusion.3 = (f16[32,384]{1,0:T(8,128)(2,1)S(1)}, f16[32,384]{1,0:T(8,128)(2,1)S(1)}, f16[32,384]{1,0:T(8,128)(2,1)S(1)}) fusion(f32[32,384]{1,0:T(8,128)} %param.7, f32[32]{0:T(128)} %param.6, f32[32,384]{1,0:T(8,128)} %param.8, f32[32,384]{1,0:T(8,128)} %param.9), kind=kLoop, calls=%fused_computation.4 | loop fusion | flops 135168 | bytes 221312 | tf_op jit(solution)/shard_map/convert_element_type | solution.py:105
  1.6 0.9 broadcast_in_dim.8
  2.5 7.6 %all-to-all-start = ((f16[8,32,1152]{2,1,0:T(8,128)(2,1)}), f16[8,32,1152]{2,1,0:T(8,128)(2,1)S(1)}, u32[]{:S(2)}, u32[]{:S(2)}) async-start(f16[8,32,1152]{2,1,0:T(8,128)(2,1)} %broadcast_in_dim.8), calls=%async_computation | async-start | bytes 1179648 | tf_op jit(solution)/shard_map/all_to_all | solution.py:107
  10.1 6.1 %collective-permute-start = (bf16[320,256]{1,0:T(8,128)(2,1)}, bf16[320,256]{1,0:T(8,128)(2,1)S(1)}, u32[]{:S(2)}, u32[]{:S(2)}) collective-permute-start(bf16[320,256]{1,0:T(8,128)(2,1)} %prompt_ref.1), channel_id=1, source_target_pairs={{0,1},{1,0},{2,3},{3,2},{4,5},{5,4},{6,7},{7,6},{8,9},{9,8},{10,11... | collective-permute-start | bytes 491528 | tf_op jit(solution)/shard_map/ppermute | solution.py:108
  16.2 0.0 copy-start.2
  16.2 0.9 %copy-done.2 = bf16[320,256]{1,0:T(8,128)(2,1)S(1)} copy-done((bf16[320,256]{1,0:T(8,128)(2,1)S(1)}, bf16[320,256]{1,0:T(8,128)(2,1)}, u32[]{:S(2)}) %copy-start.2) | copy-done | bytes 163864
  17.1 0.3 collective-permute-done.second_ref
  17.4 3.1 %collective-permute-start.1 = (bf16[2,320,256]{2,1,0:T(8,128)(2,1)S(1)}, bf16[2,320,256]{2,1,0:T(8,128)(2,1)S(1)}, u32[]{:S(2)}, u32[]{:S(2)}) collective-permute-start(bf16[2,320,256]{2,1,0:T(8,128)(2,1)S(1)} %shard_map.86.refs_0_), channel_id=1, source_target_pairs={{0,2},{1,3},{2,4},{3,5},{4,6},{5,7},{6,0},{7,1},{8,10},{9,11},{10,... | collective-permute-start | bytes 983048 | tf_op jit(solution)/shard_map/ppermute | solution.py:126
  20.6 4.4 %collective-permute-start.2 = (bf16[2,320,256]{2,1,0:T(8,128)(2,1)S(1)}, bf16[2,320,256]{2,1,0:T(8,128)(2,1)S(1)}, u32[]{:S(2)}, u32[]{:S(2)}) collective-permute-start(bf16[2,320,256]{2,1,0:T(8,128)(2,1)S(1)} %shard_map.86.refs_0_), channel_id=1, source_target_pairs={{0,4},{1,5},{2,6},{3,7},{4,0},{5,1},{6,2},{7,3},{8,12},{9,13},{10,... | collective-permute-start | bytes 983048 | tf_op jit(solution)/shard_map/ppermute | solution.py:126
  24.9 3.1 %collective-permute-start.3 = (bf16[2,320,256]{2,1,0:T(8,128)(2,1)S(1)}, bf16[2,320,256]{2,1,0:T(8,128)(2,1)S(1)}, u32[]{:S(2)}, u32[]{:S(2)}) collective-permute-start(bf16[2,320,256]{2,1,0:T(8,128)(2,1)S(1)} %shard_map.86.refs_0_), channel_id=1, source_target_pairs={{0,6},{1,7},{2,0},{3,1},{4,2},{5,3},{6,4},{7,5},{8,14},{9,15},{10,... | collective-permute-start | bytes 983048 | tf_op jit(solution)/shard_map/ppermute | solution.py:126
  28.0 0.0 all-to-all-done
  28.0 31.1 %all-gather.1 = f16[2048,1152]{1,0:T(8,128)(2,1)S(1)} all-gather(f16[256,1152]{1,0:T(8,128)(2,1)S(1)} %bitcast.6), channel_id=1, replica_groups={{0,8,16,24,32,40,48,56},{64,72,80,88,96,104,112,120},{128,136,144,152,1..., dimensions={0}, use_global_device_ids=true | all-gather | bytes 5308416 | tf_op jit(solution)/shard_map/all_gather | solution.py:127
  59.1 1.1 %multiply_convert_fusion = bf16[2048,1152]{1,0:T(8,128)(2,1)S(1)} fusion(f16[2048,1152]{1,0:T(8,128)(2,1)S(1)} %all-gather.1), kind=kLoop, calls=%fused_computation | loop fusion | flops 7077888 | bytes 9437184 | tf_op jit(solution)/shard_map/convert_element_type | solution.py:128
  60.2 0.0 collective-permute-done.1.refs_1_
  60.2 2.7 %shard_map.87 = (bf16[4,320,256]{2,1,0:T(8,128)(2,1)S(1)}, f32[4,320,256]{2,1,0:T(8,128)S(1)}) custom-call(s32[1]{0:T(128)} %bitcast.me, bf16[2,320,256]{2,1,0:T(8,128)(2,1)S(1)} %shard_map.86.refs_0_, bf16[2,320,256]{2,1,0:T(8,128)(2,1)S(1)} %collective-permute-done.1.refs_1_, bf16[2,320,256]{2,1,0:T(8,128)(2,1)S(1)} %collective-permute-done.2.refs_2_, ...), custom_call_target="tpu_custom_call" | custom-call | tf_op jit(solution)/shard_map/pallas_call | solution.py:131
  62.9 2.1 %copy-done = bf16[2048,1152]{1,0:T(8,128)(2,1)} copy-done((bf16[2048,1152]{1,0:T(8,128)(2,1)}, bf16[2048,1152]{1,0:T(8,128)(2,1)S(1)}, u32[]{:S(2)}) %copy-start) | copy-done | bytes 4718616
  65.0 5.9 %collective-permute-start.4 = (bf16[4,320,256]{2,1,0:T(8,128)(2,1)S(1)}, bf16[4,320,256]{2,1,0:T(8,128)(2,1)S(1)}, u32[]{:S(2)}, u32[]{:S(2)}) collective-permute-start(bf16[4,320,256]{2,1,0:T(8,128)(2,1)S(1)} %get-tuple-element.13), channel_id=1, source_target_pairs={{0,1},{1,0},{2,3},{3,2},{4,5},{5,4},{6,7},{7,6},{8,9},{9,8},{10,11... | collective-permute-start | bytes 1966088 | tf_op jit(solution)/shard_map/ppermute | solution.py:138
  70.9 1.7 %collective-permute-done.4.got_ref = bf16[4,320,256]{2,1,0:T(8,128)(2,1)S(1)} collective-permute-done((bf16[4,320,256]{2,1,0:T(8,128)(2,1)S(1)}, bf16[4,320,256]{2,1,0:T(8,128)(2,1)S(1)}, u32[]{:S(2)}, u32[]{:S(2)}) %collective-permute-start.4) | collective-permute-done | bytes 655392 | tf_op jit(solution)/shard_map/ppermute | solution.py:138
  72.6 1.0 %shard_map.88 = bf16[4,320,256]{2,1,0:T(8,128)(2,1)} custom-call(f32[4,320,256]{2,1,0:T(8,128)S(1)} %get-tuple-element.12.mine_ref, bf16[4,320,256]{2,1,0:T(8,128)(2,1)S(1)} %collective-permute-done.4.got_ref), custom_call_target="tpu_custom_call" | custom-call | tf_op jit(solution)/shard_map/pallas_call | solution.py:139
  73.5 3.5 %all-to-all-start.1 = ((bf16[4,320,256]{2,1,0:T(8,128)(2,1)}), bf16[4,320,256]{2,1,0:T(8,128)(2,1)S(1)}, u32[]{:S(2)}, u32[]{:S(2)}) async-start(bf16[4,320,256]{2,1,0:T(8,128)(2,1)} %shard_map.88), calls=%async_computation.1 | async-start | bytes 1310720 | tf_op jit(solution)/shard_map/all_to_all | solution.py:147
  77.0 2.3 %copy-done.1 = bf16[2048,1152]{1,0:T(8,128)(2,1)S(1)} copy-done((bf16[2048,1152]{1,0:T(8,128)(2,1)S(1)}, bf16[2048,1152]{1,0:T(8,128)(2,1)}, u32[]{:S(2)}) %copy-start.1) | copy-done | bytes 4718616
  79.4 4.0 %shard_map.84 = (bf16[384,2048]{1,0:T(8,128)(2,1)}, bf16[384,2048]{1,0:T(8,128)(2,1)}, bf16[384,2048]{1,0:T(8,128)(2,1)}) custom-call(s32[1]{0:T(128)} %bitcast.me, bf16[64,32,1152]{2,1,0:T(8,128)(2,1)S(1)} %bitcast.5), custom_call_target="tpu_custom_call" | custom-call | flops 2000000000 | bytes 9437184 | tf_op jit(solution)/shard_map/pallas_call | solution.py:150
  83.3 4.3 %all-to-all-done.1.parts_ref = bf16[4,320,256]{2,1,0:T(8,128)(2,1)S(1)} async-done(((bf16[4,320,256]{2,1,0:T(8,128)(2,1)}), bf16[4,320,256]{2,1,0:T(8,128)(2,1)S(1)}, u32[]{:S(2)}, u32[]{:S(2)}) %all-to-all-start.1) | async-done | bytes 655392 | tf_op jit(solution)/shard_map/all_to_all | solution.py:147
  87.6 0.7 shard_map.89
  (7 shorter events, 0.1 us)
Async XLA Ops:
  2.5 25.5 %all-to-all-start = ((f16[8,32,1152]{2,1,0:T(8,128)(2,1)}), f16[8,32,1152]{2,1,0:T(8,128)(2,1)S(1)}, u32[]{:S(2)}, u32[]{:S(2)}) async-start(f16[8,32,1152]{2,1,0:T(8,128)(2,1)} %broadcast_in_dim.8), calls=%async_computation | async-start | bytes 1179648 | tf_op jit(solution)/shard_map/all_to_all | solution.py:107
  10.1 7.3 %collective-permute-start = (bf16[320,256]{1,0:T(8,128)(2,1)}, bf16[320,256]{1,0:T(8,128)(2,1)S(1)}, u32[]{:S(2)}, u32[]{:S(2)}) collective-permute-start(bf16[320,256]{1,0:T(8,128)(2,1)} %prompt_ref.1), channel_id=1, source_target_pairs={{0,1},{1,0},{2,3},{3,2},{4,5},{5,4},{6,7},{7,6},{8,9},{9,8},{10,11... | collective-permute-start | bytes 491528 | tf_op jit(solution)/shard_map/ppermute | solution.py:108
  16.2 0.9 %copy-start.2 = (bf16[320,256]{1,0:T(8,128)(2,1)S(1)}, bf16[320,256]{1,0:T(8,128)(2,1)}, u32[]{:S(2)}) copy-start(bf16[320,256]{1,0:T(8,128)(2,1)} %prompt_ref.1) | copy-start | bytes 491524
  17.4 42.7 %collective-permute-start.1 = (bf16[2,320,256]{2,1,0:T(8,128)(2,1)S(1)}, bf16[2,320,256]{2,1,0:T(8,128)(2,1)S(1)}, u32[]{:S(2)}, u32[]{:S(2)}) collective-permute-start(bf16[2,320,256]{2,1,0:T(8,128)(2,1)S(1)} %shard_map.86.refs_0_), channel_id=1, source_target_pairs={{0,2},{1,3},{2,4},{3,5},{4,6},{5,7},{6,0},{7,1},{8,10},{9,11},{10,... | collective-permute-start | bytes 983048 | tf_op jit(solution)/shard_map/ppermute | solution.py:126
  20.6 39.6 %collective-permute-start.2 = (bf16[2,320,256]{2,1,0:T(8,128)(2,1)S(1)}, bf16[2,320,256]{2,1,0:T(8,128)(2,1)S(1)}, u32[]{:S(2)}, u32[]{:S(2)}) collective-permute-start(bf16[2,320,256]{2,1,0:T(8,128)(2,1)S(1)} %shard_map.86.refs_0_), channel_id=1, source_target_pairs={{0,4},{1,5},{2,6},{3,7},{4,0},{5,1},{6,2},{7,3},{8,12},{9,13},{10,... | collective-permute-start | bytes 983048 | tf_op jit(solution)/shard_map/ppermute | solution.py:126
  24.9 35.2 %collective-permute-start.3 = (bf16[2,320,256]{2,1,0:T(8,128)(2,1)S(1)}, bf16[2,320,256]{2,1,0:T(8,128)(2,1)S(1)}, u32[]{:S(2)}, u32[]{:S(2)}) collective-permute-start(bf16[2,320,256]{2,1,0:T(8,128)(2,1)S(1)} %shard_map.86.refs_0_), channel_id=1, source_target_pairs={{0,6},{1,7},{2,0},{3,1},{4,2},{5,3},{6,4},{7,5},{8,14},{9,15},{10,... | collective-permute-start | bytes 983048 | tf_op jit(solution)/shard_map/ppermute | solution.py:126
  62.9 2.1 %copy-start = (bf16[2048,1152]{1,0:T(8,128)(2,1)}, bf16[2048,1152]{1,0:T(8,128)(2,1)S(1)}, u32[]{:S(2)}) copy-start(bf16[2048,1152]{1,0:T(8,128)(2,1)S(1)} %multiply_convert_fusion) | copy-start | bytes 14155780
  65.0 7.6 %collective-permute-start.4 = (bf16[4,320,256]{2,1,0:T(8,128)(2,1)S(1)}, bf16[4,320,256]{2,1,0:T(8,128)(2,1)S(1)}, u32[]{:S(2)}, u32[]{:S(2)}) collective-permute-start(bf16[4,320,256]{2,1,0:T(8,128)(2,1)S(1)} %get-tuple-element.13), channel_id=1, source_target_pairs={{0,1},{1,0},{2,3},{3,2},{4,5},{5,4},{6,7},{7,6},{8,9},{9,8},{10,11... | collective-permute-start | bytes 1966088 | tf_op jit(solution)/shard_map/ppermute | solution.py:138
  73.5 14.1 %all-to-all-start.1 = ((bf16[4,320,256]{2,1,0:T(8,128)(2,1)}), bf16[4,320,256]{2,1,0:T(8,128)(2,1)S(1)}, u32[]{:S(2)}, u32[]{:S(2)}) async-start(bf16[4,320,256]{2,1,0:T(8,128)(2,1)} %shard_map.88), calls=%async_computation.1 | async-start | bytes 1310720 | tf_op jit(solution)/shard_map/all_to_all | solution.py:147
  77.0 2.3 %copy-start.1 = (bf16[2048,1152]{1,0:T(8,128)(2,1)S(1)}, bf16[2048,1152]{1,0:T(8,128)(2,1)}, u32[]{:S(2)}) copy-start(bf16[2048,1152]{1,0:T(8,128)(2,1)} %copy-done) | copy-start | bytes 14155780

commit v6 on v5

--- a/solution.py
+++ b/solution.py
@@ -41,16 +41,20 @@
         at = [slab * along_z + y * along_y for y in range(SIDE)]
         return jnp.concatenate([near_ref[row, :, columns] for row in at], axis=0)
 
-    squares, both = jnp.zeros((tokens, width), jnp.float32), 0.0
+    squares = jnp.zeros((tokens, width), jnp.float32)
+    for pair in pairs:
+        for k in range(2):
+            x = pair[k].astype(jnp.float32)
+            squares += x * x
+    inverse = lax.rsqrt(jnp.sum(squares, axis=1, keepdims=True) / (2 * chips * width) + 1e-06)
+    both = 0.0
     for step, pair in enumerate(pairs):
         chip = lax.rem(me[0] // 2 + chips - step, chips)
         for k in range(2):
-            x = pair[k]
+            normed = (pair[k].astype(jnp.float32) * inverse).astype(jnp.bfloat16)
             slab = 2 * chip + (core if k == 0 else 1 - core)
-            both += jnp.dot(x, weights(slab, slice(0, 2 * cols)), preferred_element_type=jnp.float32)
-            squares += x.astype(jnp.float32) * x.astype(jnp.float32)
-    inverse = lax.rsqrt(jnp.sum(squares, axis=1, keepdims=True) / (2 * chips * width) + 1e-06)
-    gate, up = both[:, :cols] * inverse, both[:, cols:] * inverse
+            both += jnp.dot(normed, weights(slab, slice(0, 2 * cols)), preferred_element_type=jnp.float32)
+    gate, up = both[:, :cols], both[:, cols:]
     hidden = (gate / (1 + jnp.exp(-gate)) * up).astype(jnp.bfloat16)
 
     def share(slab):

time: 88.9 us -> 89.1 us (level)
  transfers between devices with their start and end apart: 7 -> 7, of which waited for: 3 -> 3; matrix products, arithmetic and copies ran while one was open for 1% -> 1% of each run, Pallas kernels for 5% -> 4%
where the time goes in v6:
time: 89.1 us; the launch traced here: 88.6 us
  starting transfers between devices  33.6 us (38%)
  blocking collectives  31.1 us (35%)
  Pallas kernels  8.58 us (10%)
  waiting for transfers between devices  6.27 us (7%)
  local copies, waits for them, and re-layouts  6.22 us (7%)
  other arithmetic  2.05 us (2%)
    all_gather x1, blocking collectives, on_device(): lax.all_gather(own.reshape(SIDE * rows, 3 * cols), every, axis=0, tiled=T...  31.1 us
    ppermute x3, starting transfers between devices, on_device(): lax.ppermute(pairs[0], 'tp', [(t, (t + 2 * step) % tp) for t in range(tp)])  10.5 us
    all_to_all x1, starting transfers between devices, on_device(): lax.all_to_all(copies, every, 0, 0, tiled=True, axis_index_groups=lines(t...  7.64 us
    ppermute x1, starting transfers between devices, on_device(): partner = lax.ppermute(prompt, 'tp', [(t, t ^ 1) for t in range(tp)])  6.07 us
    ppermute x1, starting transfers between devices, on_device(): got = lax.ppermute(other, 'tp', [(t, t ^ 1) for t in range(tp)])  5.87 us
    unnamed x6, local copies, waits for them, and re-layouts  5.36 us
    all_to_all x1, waiting for transfers between devices, on_device(): lax.all_to_all(paired, 'tp', 0, 0, tiled=True, axis_index_groups=chips)  4.28 us
    pallas_call x1, Pallas kernels, on_device(): pl.pallas_call(turn_kernel, out_shape=(turned, turned, turned), grid_spec...  3.95 us
  transfers between devices with their start and end apart: 7, of which 3 were waited for; matrix products, arithmetic and copies ran while one was open for 1% of the time, Pallas kernels for 4%

profile of v6, /device:TPU:1, one launch (start us, length us, event | category | flops | bytes accessed | tf_op | source)
XLA Modules:
  0.0 88.6 jit_solution(8326951450805978560)
XLA Ops:
  0.6 0.9 %multiply_convert_fusion.3 = (f16[32,384]{1,0:T(8,128)(2,1)S(1)}, f16[32,384]{1,0:T(8,128)(2,1)S(1)}, f16[32,384]{1,0:T(8,128)(2,1)S(1)}) fusion(f32[32,384]{1,0:T(8,128)} %param.7, f32[32]{0:T(128)} %param.6, f32[32,384]{1,0:T(8,128)} %param.8, f32[32,384]{1,0:T(8,128)} %param.9), kind=kLoop, calls=%fused_computation.4 | loop fusion | flops 135168 | bytes 221312 | tf_op jit(solution)/shard_map/convert_element_type | solution.py:109
  1.6 0.9 broadcast_in_dim.8
  2.5 7.6 %all-to-all-start = ((f16[8,32,1152]{2,1,0:T(8,128)(2,1)}), f16[8,32,1152]{2,1,0:T(8,128)(2,1)S(1)}, u32[]{:S(2)}, u32[]{:S(2)}) async-start(f16[8,32,1152]{2,1,0:T(8,128)(2,1)} %broadcast_in_dim.8), calls=%async_computation | async-start | bytes 1179648 | tf_op jit(solution)/shard_map/all_to_all | solution.py:111
  10.1 6.1 %collective-permute-start = (bf16[320,256]{1,0:T(8,128)(2,1)}, bf16[320,256]{1,0:T(8,128)(2,1)S(1)}, u32[]{:S(2)}, u32[]{:S(2)}) collective-permute-start(bf16[320,256]{1,0:T(8,128)(2,1)} %prompt_ref.1), channel_id=1, source_target_pairs={{0,1},{1,0},{2,3},{3,2},{4,5},{5,4},{6,7},{7,6},{8,9},{9,8},{10,11... | collective-permute-start | bytes 491528 | tf_op jit(solution)/shard_map/ppermute | solution.py:112
  16.2 0.0 copy-start.2
  16.2 0.9 %copy-done.2 = bf16[320,256]{1,0:T(8,128)(2,1)S(1)} copy-done((bf16[320,256]{1,0:T(8,128)(2,1)S(1)}, bf16[320,256]{1,0:T(8,128)(2,1)}, u32[]{:S(2)}) %copy-start.2) | copy-done | bytes 163864
  17.1 0.3 collective-permute-done.second_ref
  17.4 3.1 %collective-permute-start.1 = (bf16[2,320,256]{2,1,0:T(8,128)(2,1)S(1)}, bf16[2,320,256]{2,1,0:T(8,128)(2,1)S(1)}, u32[]{:S(2)}, u32[]{:S(2)}) collective-permute-start(bf16[2,320,256]{2,1,0:T(8,128)(2,1)S(1)} %shard_map.86.refs_0_), channel_id=1, source_target_pairs={{0,2},{1,3},{2,4},{3,5},{4,6},{5,7},{6,0},{7,1},{8,10},{9,11},{10,... | collective-permute-start | bytes 983048 | tf_op jit(solution)/shard_map/ppermute | solution.py:130
  20.6 4.4 %collective-permute-start.2 = (bf16[2,320,256]{2,1,0:T(8,128)(2,1)S(1)}, bf16[2,320,256]{2,1,0:T(8,128)(2,1)S(1)}, u32[]{:S(2)}, u32[]{:S(2)}) collective-permute-start(bf16[2,320,256]{2,1,0:T(8,128)(2,1)S(1)} %shard_map.86.refs_0_), channel_id=1, source_target_pairs={{0,4},{1,5},{2,6},{3,7},{4,0},{5,1},{6,2},{7,3},{8,12},{9,13},{10,... | collective-permute-start | bytes 983048 | tf_op jit(solution)/shard_map/ppermute | solution.py:130
  24.9 3.1 %collective-permute-start.3 = (bf16[2,320,256]{2,1,0:T(8,128)(2,1)S(1)}, bf16[2,320,256]{2,1,0:T(8,128)(2,1)S(1)}, u32[]{:S(2)}, u32[]{:S(2)}) collective-permute-start(bf16[2,320,256]{2,1,0:T(8,128)(2,1)S(1)} %shard_map.86.refs_0_), channel_id=1, source_target_pairs={{0,6},{1,7},{2,0},{3,1},{4,2},{5,3},{6,4},{7,5},{8,14},{9,15},{10,... | collective-permute-start | bytes 983048 | tf_op jit(solution)/shard_map/ppermute | solution.py:130
  28.0 0.0 all-to-all-done
  28.0 31.1 %all-gather.1 = f16[2048,1152]{1,0:T(8,128)(2,1)S(1)} all-gather(f16[256,1152]{1,0:T(8,128)(2,1)S(1)} %bitcast.6), channel_id=1, replica_groups={{0,8,16,24,32,40,48,56},{64,72,80,88,96,104,112,120},{128,136,144,152,1..., dimensions={0}, use_global_device_ids=true | all-gather | bytes 5308416 | tf_op jit(solution)/shard_map/all_gather | solution.py:131
  59.1 1.1 %multiply_convert_fusion = bf16[2048,1152]{1,0:T(8,128)(2,1)S(1)} fusion(f16[2048,1152]{1,0:T(8,128)(2,1)S(1)} %all-gather.1), kind=kLoop, calls=%fused_computation | loop fusion | flops 7077888 | bytes 9437184 | tf_op jit(solution)/shard_map/convert_element_type | solution.py:132
  60.2 0.0 collective-permute-done.1.refs_1_
  60.2 2.9 %shard_map.87 = (bf16[4,320,256]{2,1,0:T(8,128)(2,1)S(1)}, f32[4,320,256]{2,1,0:T(8,128)S(1)}) custom-call(s32[1]{0:T(128)} %bitcast.me, bf16[2,320,256]{2,1,0:T(8,128)(2,1)S(1)} %shard_map.86.refs_0_, bf16[2,320,256]{2,1,0:T(8,128)(2,1)S(1)} %collective-permute-done.1.refs_1_, bf16[2,320,256]{2,1,0:T(8,128)(2,1)S(1)} %collective-permute-done.2.refs_2_, ...), custom_call_target="tpu_custom_call" | custom-call | tf_op jit(solution)/shard_map/pallas_call | solution.py:135
  63.1 2.1 %copy-done = bf16[2048,1152]{1,0:T(8,128)(2,1)} copy-done((bf16[2048,1152]{1,0:T(8,128)(2,1)}, bf16[2048,1152]{1,0:T(8,128)(2,1)S(1)}, u32[]{:S(2)}) %copy-start) | copy-done | bytes 4718616
  65.2 5.9 %collective-permute-start.4 = (bf16[4,320,256]{2,1,0:T(8,128)(2,1)S(1)}, bf16[4,320,256]{2,1,0:T(8,128)(2,1)S(1)}, u32[]{:S(2)}, u32[]{:S(2)}) collective-permute-start(bf16[4,320,256]{2,1,0:T(8,128)(2,1)S(1)} %get-tuple-element.13), channel_id=1, source_target_pairs={{0,1},{1,0},{2,3},{3,2},{4,5},{5,4},{6,7},{7,6},{8,9},{9,8},{10,11... | collective-permute-start | bytes 1966088 | tf_op jit(solution)/shard_map/ppermute | solution.py:142
  71.1 1.7 %collective-permute-done.4.got_ref = bf16[4,320,256]{2,1,0:T(8,128)(2,1)S(1)} collective-permute-done((bf16[4,320,256]{2,1,0:T(8,128)(2,1)S(1)}, bf16[4,320,256]{2,1,0:T(8,128)(2,1)S(1)}, u32[]{:S(2)}, u32[]{:S(2)}) %collective-permute-start.4) | collective-permute-done | bytes 655392 | tf_op jit(solution)/shard_map/ppermute | solution.py:142
  72.8 1.0 %shard_map.88 = bf16[4,320,256]{2,1,0:T(8,128)(2,1)} custom-call(f32[4,320,256]{2,1,0:T(8,128)S(1)} %get-tuple-element.12.mine_ref, bf16[4,320,256]{2,1,0:T(8,128)(2,1)S(1)} %collective-permute-done.4.got_ref), custom_call_target="tpu_custom_call" | custom-call | tf_op jit(solution)/shard_map/pallas_call | solution.py:143
  73.8 3.5 %all-to-all-start.1 = ((bf16[4,320,256]{2,1,0:T(8,128)(2,1)}), bf16[4,320,256]{2,1,0:T(8,128)(2,1)S(1)}, u32[]{:S(2)}, u32[]{:S(2)}) async-start(bf16[4,320,256]{2,1,0:T(8,128)(2,1)} %shard_map.88), calls=%async_computation.1 | async-start | bytes 1310720 | tf_op jit(solution)/shard_map/all_to_all | solution.py:151
  77.3 2.3 %copy-done.1 = bf16[2048,1152]{1,0:T(8,128)(2,1)S(1)} copy-done((bf16[2048,1152]{1,0:T(8,128)(2,1)S(1)}, bf16[2048,1152]{1,0:T(8,128)(2,1)}, u32[]{:S(2)}) %copy-start.1) | copy-done | bytes 4718616
  79.6 4.0 %shard_map.84 = (bf16[384,2048]{1,0:T(8,128)(2,1)}, bf16[384,2048]{1,0:T(8,128)(2,1)}, bf16[384,2048]{1,0:T(8,128)(2,1)}) custom-call(s32[1]{0:T(128)} %bitcast.me, bf16[64,32,1152]{2,1,0:T(8,128)(2,1)S(1)} %bitcast.5), custom_call_target="tpu_custom_call" | custom-call | flops 2000000000 | bytes 9437184 | tf_op jit(solution)/shard_map/pallas_call | solution.py:154
  83.5 4.3 %all-to-all-done.1.parts_ref = bf16[4,320,256]{2,1,0:T(8,128)(2,1)S(1)} async-done(((bf16[4,320,256]{2,1,0:T(8,128)(2,1)}), bf16[4,320,256]{2,1,0:T(8,128)(2,1)S(1)}, u32[]{:S(2)}, u32[]{:S(2)}) %all-to-all-start.1) | async-done | bytes 655392 | tf_op jit(solution)/shard_map/all_to_all | solution.py:151
  87.8 0.7 shard_map.89
  (7 shorter events, 0.1 us)
Async XLA Ops:
  2.5 25.5 %all-to-all-start = ((f16[8,32,1152]{2,1,0:T(8,128)(2,1)}), f16[8,32,1152]{2,1,0:T(8,128)(2,1)S(1)}, u32[]{:S(2)}, u32[]{:S(2)}) async-start(f16[8,32,1152]{2,1,0:T(8,128)(2,1)} %broadcast_in_dim.8), calls=%async_computation | async-start | bytes 1179648 | tf_op jit(solution)/shard_map/all_to_all | solution.py:111
  10.1 7.3 %collective-permute-start = (bf16[320,256]{1,0:T(8,128)(2,1)}, bf16[320,256]{1,0:T(8,128)(2,1)S(1)}, u32[]{:S(2)}, u32[]{:S(2)}) collective-permute-start(bf16[320,256]{1,0:T(8,128)(2,1)} %prompt_ref.1), channel_id=1, source_target_pairs={{0,1},{1,0},{2,3},{3,2},{4,5},{5,4},{6,7},{7,6},{8,9},{9,8},{10,11... | collective-permute-start | bytes 491528 | tf_op jit(solution)/shard_map/ppermute | solution.py:112
  16.2 0.9 %copy-start.2 = (bf16[320,256]{1,0:T(8,128)(2,1)S(1)}, bf16[320,256]{1,0:T(8,128)(2,1)}, u32[]{:S(2)}) copy-start(bf16[320,256]{1,0:T(8,128)(2,1)} %prompt_ref.1) | copy-start | bytes 491524
  17.4 42.7 %collective-permute-start.1 = (bf16[2,320,256]{2,1,0:T(8,128)(2,1)S(1)}, bf16[2,320,256]{2,1,0:T(8,128)(2,1)S(1)}, u32[]{:S(2)}, u32[]{:S(2)}) collective-permute-start(bf16[2,320,256]{2,1,0:T(8,128)(2,1)S(1)} %shard_map.86.refs_0_), channel_id=1, source_target_pairs={{0,2},{1,3},{2,4},{3,5},{4,6},{5,7},{6,0},{7,1},{8,10},{9,11},{10,... | collective-permute-start | bytes 983048 | tf_op jit(solution)/shard_map/ppermute | solution.py:130
  20.6 39.6 %collective-permute-start.2 = (bf16[2,320,256]{2,1,0:T(8,128)(2,1)S(1)}, bf16[2,320,256]{2,1,0:T(8,128)(2,1)S(1)}, u32[]{:S(2)}, u32[]{:S(2)}) collective-permute-start(bf16[2,320,256]{2,1,0:T(8,128)(2,1)S(1)} %shard_map.86.refs_0_), channel_id=1, source_target_pairs={{0,4},{1,5},{2,6},{3,7},{4,0},{5,1},{6,2},{7,3},{8,12},{9,13},{10,... | collective-permute-start | bytes 983048 | tf_op jit(solution)/shard_map/ppermute | solution.py:130
  24.9 35.2 %collective-permute-start.3 = (bf16[2,320,256]{2,1,0:T(8,128)(2,1)S(1)}, bf16[2,320,256]{2,1,0:T(8,128)(2,1)S(1)}, u32[]{:S(2)}, u32[]{:S(2)}) collective-permute-start(bf16[2,320,256]{2,1,0:T(8,128)(2,1)S(1)} %shard_map.86.refs_0_), channel_id=1, source_target_pairs={{0,6},{1,7},{2,0},{3,1},{4,2},{5,3},{6,4},{7,5},{8,14},{9,15},{10,... | collective-permute-start | bytes 983048 | tf_op jit(solution)/shard_map/ppermute | solution.py:130
  63.1 2.1 %copy-start = (bf16[2048,1152]{1,0:T(8,128)(2,1)}, bf16[2048,1152]{1,0:T(8,128)(2,1)S(1)}, u32[]{:S(2)}) copy-start(bf16[2048,1152]{1,0:T(8,128)(2,1)S(1)} %multiply_convert_fusion) | copy-start | bytes 14155780
  65.2 7.6 %collective-permute-start.4 = (bf16[4,320,256]{2,1,0:T(8,128)(2,1)S(1)}, bf16[4,320,256]{2,1,0:T(8,128)(2,1)S(1)}, u32[]{:S(2)}, u32[]{:S(2)}) collective-permute-start(bf16[4,320,256]{2,1,0:T(8,128)(2,1)S(1)} %get-tuple-element.13), channel_id=1, source_target_pairs={{0,1},{1,0},{2,3},{3,2},{4,5},{5,4},{6,7},{7,6},{8,9},{9,8},{10,11... | collective-permute-start | bytes 1966088 | tf_op jit(solution)/shard_map/ppermute | solution.py:142
  73.8 14.1 %all-to-all-start.1 = ((bf16[4,320,256]{2,1,0:T(8,128)(2,1)}), bf16[4,320,256]{2,1,0:T(8,128)(2,1)S(1)}, u32[]{:S(2)}, u32[]{:S(2)}) async-start(bf16[4,320,256]{2,1,0:T(8,128)(2,1)} %shard_map.88), calls=%async_computation.1 | async-start | bytes 1310720 | tf_op jit(solution)/shard_map/all_to_all | solution.py:151
  77.2 2.3 %copy-start.1 = (bf16[2048,1152]{1,0:T(8,128)(2,1)S(1)}, bf16[2048,1152]{1,0:T(8,128)(2,1)}, u32[]{:S(2)}) copy-start(bf16[2048,1152]{1,0:T(8,128)(2,1)} %copy-done) | copy-start | bytes 14155780

commit v7 on v6

--- a/solution.py
+++ b/solution.py
@@ -7,6 +7,7 @@
 
 
 SIDE = 8
+SLABS = 4
 SCALE = 2.0**18
 VMEM = pl.BlockSpec(memory_space=pltpu.VMEM)
 SMEM = pl.BlockSpec(memory_space=pltpu.SMEM)
@@ -73,7 +74,8 @@
 def turn_kernel(me, near_ref, *outs):
     cols = outs[0].shape[0]
     along_z, along_y = strides(lax.rem(me[0], 2))
-    at = [pl.program_id(0) * along_z + y * along_y for y in range(SIDE)]
+    zs = [pl.program_id(0) * SLABS + k for k in range(SLABS)]
+    at = [z * along_z + y * along_y for z in zs for y in range(SIDE)]
     for k, out in enumerate(outs):
         slab = jnp.concatenate([near_ref[row, :, k * cols : (k + 1) * cols] for row in at], axis=0)
         out[...] = slab.T
@@ -156,9 +158,9 @@
         out_shape=(turned, turned, turned),
         grid_spec=pltpu.PrefetchScalarGridSpec(
             num_scalar_prefetch=1,
-            grid=(SIDE,),
+            grid=(SIDE // SLABS,),
             in_specs=[VMEM],
-            out_specs=[pl.BlockSpec((cols, SIDE * rows), lambda z, me: (0, z))] * 3,
+            out_specs=[pl.BlockSpec((cols, SLABS * SIDE * rows), lambda z, me: (0, z))] * 3,
         ),
         compiler_params=pltpu.CompilerParams(vmem_limit_bytes=16 << 20),
         cost_estimate=pl.CostEstimate(flops=2 * 10**9, bytes_accessed=12 * rows * fs * cols, transcendentals=0),

time: 89.1 us -> 89.1 us (level)
  waiting for transfers between devices: 6.27 us -> 7.46 us
  Pallas kernels: 8.58 us -> 7.4 us
    pallas_call x1, Pallas kernels: 3.95 us -> 2.76 us  [on_device(): pl.pallas_call(turn_kernel, out_shape=(turned, turned, turned), grid_spec...]
    all_to_all x1, waiting for transfers between devices: 4.28 us -> 5.47 us  [on_device(): lax.all_to_all(paired, 'tp', 0, 0, tiled=True, axis_index_groups=chips)]
  transfers between devices with their start and end apart: 7 -> 7, of which waited for: 3 -> 3; matrix products, arithmetic and copies ran while one was open for 1% -> 1% of each run, Pallas kernels for 4% -> 3%
where the time goes in v7:
time: 89.1 us; the launch traced here: 88.6 us
  starting transfers between devices  33.6 us (38%)
  blocking collectives  31.1 us (35%)
  waiting for transfers between devices  7.46 us (8%)
  Pallas kernels  7.4 us (8%)
  local copies, waits for them, and re-layouts  6.22 us (7%)
  other arithmetic  2.05 us (2%)
    all_gather x1, blocking collectives, on_device(): lax.all_gather(own.reshape(SIDE * rows, 3 * cols), every, axis=0, tiled=T...  31.1 us
    ppermute x3, starting transfers between devices, on_device(): lax.ppermute(pairs[0], 'tp', [(t, (t + 2 * step) % tp) for t in range(tp)])  10.5 us
    all_to_all x1, starting transfers between devices, on_device(): lax.all_to_all(copies, every, 0, 0, tiled=True, axis_index_groups=lines(t...  7.64 us
    ppermute x1, starting transfers between devices, on_device(): partner = lax.ppermute(prompt, 'tp', [(t, t ^ 1) for t in range(tp)])  6.07 us
    ppermute x1, starting transfers between devices, on_device(): got = lax.ppermute(other, 'tp', [(t, t ^ 1) for t in range(tp)])  5.87 us
    all_to_all x1, waiting for transfers between devices, on_device(): lax.all_to_all(paired, 'tp', 0, 0, tiled=True, axis_index_groups=chips)  5.47 us
    unnamed x6, local copies, waits for them, and re-layouts  5.36 us
    all_to_all x1, starting transfers between devices, on_device(): lax.all_to_all(paired, 'tp', 0, 0, tiled=True, axis_index_groups=chips)  3.48 us
  transfers between devices with their start and end apart: 7, of which 3 were waited for; matrix products, arithmetic and copies ran while one was open for 1% of the time, Pallas kernels for 3%

profile of v7, /device:TPU:1, one launch (start us, length us, event | category | flops | bytes accessed | tf_op | source)
XLA Modules:
  0.0 88.6 jit_solution(8541828562574417808)
XLA Ops:
  0.6 0.9 %multiply_convert_fusion.3 = (f16[32,384]{1,0:T(8,128)(2,1)S(1)}, f16[32,384]{1,0:T(8,128)(2,1)S(1)}, f16[32,384]{1,0:T(8,128)(2,1)S(1)}) fusion(f32[32,384]{1,0:T(8,128)} %param.7, f32[32]{0:T(128)} %param.6, f32[32,384]{1,0:T(8,128)} %param.8, f32[32,384]{1,0:T(8,128)} %param.9), kind=kLoop, calls=%fused_computation.4 | loop fusion | flops 135168 | bytes 221312 | tf_op jit(solution)/shard_map/convert_element_type | solution.py:111
  1.6 0.9 broadcast_in_dim.8
  2.5 7.6 %all-to-all-start = ((f16[8,32,1152]{2,1,0:T(8,128)(2,1)}), f16[8,32,1152]{2,1,0:T(8,128)(2,1)S(1)}, u32[]{:S(2)}, u32[]{:S(2)}) async-start(f16[8,32,1152]{2,1,0:T(8,128)(2,1)} %broadcast_in_dim.8), calls=%async_computation | async-start | bytes 1179648 | tf_op jit(solution)/shard_map/all_to_all | solution.py:113
  10.1 6.1 %collective-permute-start = (bf16[320,256]{1,0:T(8,128)(2,1)}, bf16[320,256]{1,0:T(8,128)(2,1)S(1)}, u32[]{:S(2)}, u32[]{:S(2)}) collective-permute-start(bf16[320,256]{1,0:T(8,128)(2,1)} %prompt_ref.1), channel_id=1, source_target_pairs={{0,1},{1,0},{2,3},{3,2},{4,5},{5,4},{6,7},{7,6},{8,9},{9,8},{10,11... | collective-permute-start | bytes 491528 | tf_op jit(solution)/shard_map/ppermute | solution.py:114
  16.2 0.0 copy-start.2
  16.2 0.9 %copy-done.2 = bf16[320,256]{1,0:T(8,128)(2,1)S(1)} copy-done((bf16[320,256]{1,0:T(8,128)(2,1)S(1)}, bf16[320,256]{1,0:T(8,128)(2,1)}, u32[]{:S(2)}) %copy-start.2) | copy-done | bytes 163864
  17.1 0.3 collective-permute-done.second_ref
  17.4 3.1 %collective-permute-start.1 = (bf16[2,320,256]{2,1,0:T(8,128)(2,1)S(1)}, bf16[2,320,256]{2,1,0:T(8,128)(2,1)S(1)}, u32[]{:S(2)}, u32[]{:S(2)}) collective-permute-start(bf16[2,320,256]{2,1,0:T(8,128)(2,1)S(1)} %shard_map.86.refs_0_), channel_id=1, source_target_pairs={{0,2},{1,3},{2,4},{3,5},{4,6},{5,7},{6,0},{7,1},{8,10},{9,11},{10,... | collective-permute-start | bytes 983048 | tf_op jit(solution)/shard_map/ppermute | solution.py:132
  20.6 4.4 %collective-permute-start.2 = (bf16[2,320,256]{2,1,0:T(8,128)(2,1)S(1)}, bf16[2,320,256]{2,1,0:T(8,128)(2,1)S(1)}, u32[]{:S(2)}, u32[]{:S(2)}) collective-permute-start(bf16[2,320,256]{2,1,0:T(8,128)(2,1)S(1)} %shard_map.86.refs_0_), channel_id=1, source_target_pairs={{0,4},{1,5},{2,6},{3,7},{4,0},{5,1},{6,2},{7,3},{8,12},{9,13},{10,... | collective-permute-start | bytes 983048 | tf_op jit(solution)/shard_map/ppermute | solution.py:132
  24.9 3.1 %collective-permute-start.3 = (bf16[2,320,256]{2,1,0:T(8,128)(2,1)S(1)}, bf16[2,320,256]{2,1,0:T(8,128)(2,1)S(1)}, u32[]{:S(2)}, u32[]{:S(2)}) collective-permute-start(bf16[2,320,256]{2,1,0:T(8,128)(2,1)S(1)} %shard_map.86.refs_0_), channel_id=1, source_target_pairs={{0,6},{1,7},{2,0},{3,1},{4,2},{5,3},{6,4},{7,5},{8,14},{9,15},{10,... | collective-permute-start | bytes 983048 | tf_op jit(solution)/shard_map/ppermute | solution.py:132
  28.0 0.0 all-to-all-done
  28.0 31.1 %all-gather.1 = f16[2048,1152]{1,0:T(8,128)(2,1)S(1)} all-gather(f16[256,1152]{1,0:T(8,128)(2,1)S(1)} %bitcast.6), channel_id=1, replica_groups={{0,8,16,24,32,40,48,56},{64,72,80,88,96,104,112,120},{128,136,144,152,1..., dimensions={0}, use_global_device_ids=true | all-gather | bytes 5308416 | tf_op jit(solution)/shard_map/all_gather | solution.py:133
  59.1 1.1 %multiply_convert_fusion = bf16[2048,1152]{1,0:T(8,128)(2,1)S(1)} fusion(f16[2048,1152]{1,0:T(8,128)(2,1)S(1)} %all-gather.1), kind=kLoop, calls=%fused_computation | loop fusion | flops 7077888 | bytes 9437184 | tf_op jit(solution)/shard_map/convert_element_type | solution.py:134
  60.2 0.0 collective-permute-done.1.refs_1_
  60.2 2.9 %shard_map.87 = (bf16[4,320,256]{2,1,0:T(8,128)(2,1)S(1)}, f32[4,320,256]{2,1,0:T(8,128)S(1)}) custom-call(s32[1]{0:T(128)} %bitcast.me, bf16[2,320,256]{2,1,0:T(8,128)(2,1)S(1)} %shard_map.86.refs_0_, bf16[2,320,256]{2,1,0:T(8,128)(2,1)S(1)} %collective-permute-done.1.refs_1_, bf16[2,320,256]{2,1,0:T(8,128)(2,1)S(1)} %collective-permute-done.2.refs_2_, ...), custom_call_target="tpu_custom_call" | custom-call | tf_op jit(solution)/shard_map/pallas_call | solution.py:137
  63.1 2.1 %copy-done = bf16[2048,1152]{1,0:T(8,128)(2,1)} copy-done((bf16[2048,1152]{1,0:T(8,128)(2,1)}, bf16[2048,1152]{1,0:T(8,128)(2,1)S(1)}, u32[]{:S(2)}) %copy-start) | copy-done | bytes 4718616
  65.2 5.9 %collective-permute-start.4 = (bf16[4,320,256]{2,1,0:T(8,128)(2,1)S(1)}, bf16[4,320,256]{2,1,0:T(8,128)(2,1)S(1)}, u32[]{:S(2)}, u32[]{:S(2)}) collective-permute-start(bf16[4,320,256]{2,1,0:T(8,128)(2,1)S(1)} %get-tuple-element.13), channel_id=1, source_target_pairs={{0,1},{1,0},{2,3},{3,2},{4,5},{5,4},{6,7},{7,6},{8,9},{9,8},{10,11... | collective-permute-start | bytes 1966088 | tf_op jit(solution)/shard_map/ppermute | solution.py:144
  71.1 1.7 %collective-permute-done.4.got_ref = bf16[4,320,256]{2,1,0:T(8,128)(2,1)S(1)} collective-permute-done((bf16[4,320,256]{2,1,0:T(8,128)(2,1)S(1)}, bf16[4,320,256]{2,1,0:T(8,128)(2,1)S(1)}, u32[]{:S(2)}, u32[]{:S(2)}) %collective-permute-start.4) | collective-permute-done | bytes 655392 | tf_op jit(solution)/shard_map/ppermute | solution.py:144
  72.8 1.0 %shard_map.88 = bf16[4,320,256]{2,1,0:T(8,128)(2,1)} custom-call(f32[4,320,256]{2,1,0:T(8,128)S(1)} %get-tuple-element.12.mine_ref, bf16[4,320,256]{2,1,0:T(8,128)(2,1)S(1)} %collective-permute-done.4.got_ref), custom_call_target="tpu_custom_call" | custom-call | tf_op jit(solution)/shard_map/pallas_call | solution.py:145
  73.8 3.5 %all-to-all-start.1 = ((bf16[4,320,256]{2,1,0:T(8,128)(2,1)}), bf16[4,320,256]{2,1,0:T(8,128)(2,1)S(1)}, u32[]{:S(2)}, u32[]{:S(2)}) async-start(bf16[4,320,256]{2,1,0:T(8,128)(2,1)} %shard_map.88), calls=%async_computation.1 | async-start | bytes 1310720 | tf_op jit(solution)/shard_map/all_to_all | solution.py:153
  77.3 2.3 %copy-done.1 = bf16[2048,1152]{1,0:T(8,128)(2,1)S(1)} copy-done((bf16[2048,1152]{1,0:T(8,128)(2,1)S(1)}, bf16[2048,1152]{1,0:T(8,128)(2,1)}, u32[]{:S(2)}) %copy-start.1) | copy-done | bytes 4718616
  79.6 2.8 %shard_map.84 = (bf16[384,2048]{1,0:T(8,128)(2,1)}, bf16[384,2048]{1,0:T(8,128)(2,1)}, bf16[384,2048]{1,0:T(8,128)(2,1)}) custom-call(s32[1]{0:T(128)} %bitcast.me, bf16[64,32,1152]{2,1,0:T(8,128)(2,1)S(1)} %bitcast.5), custom_call_target="tpu_custom_call" | custom-call | flops 2000000000 | bytes 9437184 | tf_op jit(solution)/shard_map/pallas_call | solution.py:156
  82.3 5.5 %all-to-all-done.1.parts_ref = bf16[4,320,256]{2,1,0:T(8,128)(2,1)S(1)} async-done(((bf16[4,320,256]{2,1,0:T(8,128)(2,1)}), bf16[4,320,256]{2,1,0:T(8,128)(2,1)S(1)}, u32[]{:S(2)}, u32[]{:S(2)}) %all-to-all-start.1) | async-done | bytes 655392 | tf_op jit(solution)/shard_map/all_to_all | solution.py:153
  87.8 0.7 shard_map.89
  (7 shorter events, 0.1 us)
Async XLA Ops:
  2.5 25.5 %all-to-all-start = ((f16[8,32,1152]{2,1,0:T(8,128)(2,1)}), f16[8,32,1152]{2,1,0:T(8,128)(2,1)S(1)}, u32[]{:S(2)}, u32[]{:S(2)}) async-start(f16[8,32,1152]{2,1,0:T(8,128)(2,1)} %broadcast_in_dim.8), calls=%async_computation | async-start | bytes 1179648 | tf_op jit(solution)/shard_map/all_to_all | solution.py:113
  10.1 7.3 %collective-permute-start = (bf16[320,256]{1,0:T(8,128)(2,1)}, bf16[320,256]{1,0:T(8,128)(2,1)S(1)}, u32[]{:S(2)}, u32[]{:S(2)}) collective-permute-start(bf16[320,256]{1,0:T(8,128)(2,1)} %prompt_ref.1), channel_id=1, source_target_pairs={{0,1},{1,0},{2,3},{3,2},{4,5},{5,4},{6,7},{7,6},{8,9},{9,8},{10,11... | collective-permute-start | bytes 491528 | tf_op jit(solution)/shard_map/ppermute | solution.py:114
  16.2 0.9 %copy-start.2 = (bf16[320,256]{1,0:T(8,128)(2,1)S(1)}, bf16[320,256]{1,0:T(8,128)(2,1)}, u32[]{:S(2)}) copy-start(bf16[320,256]{1,0:T(8,128)(2,1)} %prompt_ref.1) | copy-start | bytes 491524
  17.4 42.7 %collective-permute-start.1 = (bf16[2,320,256]{2,1,0:T(8,128)(2,1)S(1)}, bf16[2,320,256]{2,1,0:T(8,128)(2,1)S(1)}, u32[]{:S(2)}, u32[]{:S(2)}) collective-permute-start(bf16[2,320,256]{2,1,0:T(8,128)(2,1)S(1)} %shard_map.86.refs_0_), channel_id=1, source_target_pairs={{0,2},{1,3},{2,4},{3,5},{4,6},{5,7},{6,0},{7,1},{8,10},{9,11},{10,... | collective-permute-start | bytes 983048 | tf_op jit(solution)/shard_map/ppermute | solution.py:132
  20.6 39.6 %collective-permute-start.2 = (bf16[2,320,256]{2,1,0:T(8,128)(2,1)S(1)}, bf16[2,320,256]{2,1,0:T(8,128)(2,1)S(1)}, u32[]{:S(2)}, u32[]{:S(2)}) collective-permute-start(bf16[2,320,256]{2,1,0:T(8,128)(2,1)S(1)} %shard_map.86.refs_0_), channel_id=1, source_target_pairs={{0,4},{1,5},{2,6},{3,7},{4,0},{5,1},{6,2},{7,3},{8,12},{9,13},{10,... | collective-permute-start | bytes 983048 | tf_op jit(solution)/shard_map/ppermute | solution.py:132
  24.9 35.2 %collective-permute-start.3 = (bf16[2,320,256]{2,1,0:T(8,128)(2,1)S(1)}, bf16[2,320,256]{2,1,0:T(8,128)(2,1)S(1)}, u32[]{:S(2)}, u32[]{:S(2)}) collective-permute-start(bf16[2,320,256]{2,1,0:T(8,128)(2,1)S(1)} %shard_map.86.refs_0_), channel_id=1, source_target_pairs={{0,6},{1,7},{2,0},{3,1},{4,2},{5,3},{6,4},{7,5},{8,14},{9,15},{10,... | collective-permute-start | bytes 983048 | tf_op jit(solution)/shard_map/ppermute | solution.py:132
  63.1 2.1 %copy-start = (bf16[2048,1152]{1,0:T(8,128)(2,1)}, bf16[2048,1152]{1,0:T(8,128)(2,1)S(1)}, u32[]{:S(2)}) copy-start(bf16[2048,1152]{1,0:T(8,128)(2,1)S(1)} %multiply_convert_fusion) | copy-start | bytes 14155780
  65.2 7.6 %collective-permute-start.4 = (bf16[4,320,256]{2,1,0:T(8,128)(2,1)S(1)}, bf16[4,320,256]{2,1,0:T(8,128)(2,1)S(1)}, u32[]{:S(2)}, u32[]{:S(2)}) collective-permute-start(bf16[4,320,256]{2,1,0:T(8,128)(2,1)S(1)} %get-tuple-element.13), channel_id=1, source_target_pairs={{0,1},{1,0},{2,3},{3,2},{4,5},{5,4},{6,7},{7,6},{8,9},{9,8},{10,11... | collective-permute-start | bytes 1966088 | tf_op jit(solution)/shard_map/ppermute | solution.py:144
  73.8 14.1 %all-to-all-start.1 = ((bf16[4,320,256]{2,1,0:T(8,128)(2,1)}), bf16[4,320,256]{2,1,0:T(8,128)(2,1)S(1)}, u32[]{:S(2)}, u32[]{:S(2)}) async-start(bf16[4,320,256]{2,1,0:T(8,128)(2,1)} %shard_map.88), calls=%async_computation.1 | async-start | bytes 1310720 | tf_op jit(solution)/shard_map/all_to_all | solution.py:153
  77.2 2.3 %copy-start.1 = (bf16[2048,1152]{1,0:T(8,128)(2,1)S(1)}, bf16[2048,1152]{1,0:T(8,128)(2,1)}, u32[]{:S(2)}) copy-start(bf16[2048,1152]{1,0:T(8,128)(2,1)} %copy-done) | copy-start | bytes 14155780
